TPU v7x, 128 devices: a whole 4x4x4 slice. The times are simulated.
128 devices in a mesh: ep: 64 (over z, y, x), tp: 2 (over core).
Axes of the slice: x: 4, y: 4, z: 4, core: 2. Of those that a mesh axis runs over, the one named last changes fastest.
Arguments:
- hidden_in: bfloat16 [2048, 2048], P('ep'), may hold values from -6 to 6
- past_lengths: int32 [2048], P('ep'), may hold values from 1 to 1023, as said below
- key_cache: bfloat16 [2048, 1024, 256], P('ep', None, 'tp'), may hold values from -512 to 512
- value_cache: bfloat16 [2048, 1024, 256], P('ep', None, 'tp'), may hold values from -6 to 6
- attn_gain: float32 [2048], replicated, may hold values from 0.1 to 1.9
- w_query: bfloat16 [2048, 2048], P(None, 'tp'), may hold values from -0.125 to 0.125
- w_key: bfloat16 [2048, 256], P(None, 'tp'), may hold values from -0.125 to 0.125
- w_value: bfloat16 [2048, 256], P(None, 'tp'), may hold values from -0.125 to 0.125
- lambdas: float32 [16], P('tp'), may hold values from 0.3 to 0.8
- head_gain: float32 [128], replicated, may hold values from 0.1 to 1.9
- w_out: bfloat16 [2048, 2048], P('tp'), may hold values from -0.125 to 0.125
- ffn_gain: float32 [2048], replicated, may hold values from 0.1 to 1.9
- route_ids: int32 [2048, 2], P('ep'), may hold values from 0 to 31, all different within a row; in each aligned block of 32 rows (0 to 31, 32 to 63, ...) at most 4 rows name the same one
- route_weights: float32 [2048, 2], P('ep'), may hold values from 0.2 to 1
- expert_gate: bfloat16 [64, 2048, 704], P('ep', None, 'tp'), may hold values from -0.125 to 0.125
- expert_up: bfloat16 [64, 2048, 704], P('ep', None, 'tp'), may hold values from -0.125 to 0.125
- expert_down: bfloat16 [64, 704, 2048], P('ep', None, 'tp'), may hold values from -1.25 to 1.25
- gate_vector: bfloat16 [2048], replicated, may hold values from -0.125 to 0.125
- dense_gate: bfloat16 [2048, 5632], P(None, ('ep', 'tp')), may hold values from -0.125 to 0.125
- dense_up: bfloat16 [2048, 5632], P(None, ('ep', 'tp')), may hold values from -0.125 to 0.125
- dense_down: bfloat16 [5632, 2048], P('ep', 'tp'), may hold values from -0.625 to 0.625
Outputs:
- mixed_out: bfloat16 [2048, 2048], P('ep', 'tp')
- new_keys: bfloat16 [2048, 256], P('ep', 'tp')
- new_values: bfloat16 [2048, 256], P('ep', 'tp')
Inputs may be any that keep to these rules, and one draw needn't show every extreme that they name: `past_lengths`: the new token of a sequence stands at this position; some sequence has 1023 cached positions in every draw. `route_ids`: each row names 2 different experts; among the rows of one index of ep no expert is named more than 4 times, a bound that some block reaches in every draw.
All inputs are finite; a program needn't handle non-finite values.
Results may differ from a plain program's by a relative error of at most 0.02.
The roundings to bfloat16 on the way count: a program that leaves them out, or rounds other values in their place, can miss the bound.
Values may be sent and summed in bfloat16 or wider, within the bound.
A program may use at most 128 MiB of HBM per device.

v0:
```python
import jax
import jax.numpy as jnp
from jax import lax
from jax.sharding import PartitionSpec as P

HEAD_DIM = 64
VALUE_DIM = 128


norm_eps = 1e-05
rope_base = 10000.0


def sent_to_all(x, axis):
    size = lax.axis_size(axis)
    return lax.all_to_all(jnp.broadcast_to(x[None], (size, *x.shape)), axis, 0, 0, tiled=True)


def taken_together(x, axis):
    return sent_to_all(x, axis).astype(jnp.float32).sum(axis=0)


def in_order(pieces, dim):
    pieces = jnp.moveaxis(pieces, 0, dim)
    shape = pieces.shape
    return pieces.reshape(*shape[:dim], shape[dim] * shape[dim + 1], *shape[dim + 2 :])


def collect(x, axis, dim):
    pieces = sent_to_all(x, axis)
    return in_order(pieces, dim)


def in_one_piece(arrays, axis, dim, along):
    columns = [a.reshape(*a.shape[:along], -1) for a in arrays]
    both = jnp.concatenate(columns, axis=along)
    filled, at, outs = (lax.all_gather(both, axis, axis=dim, tiled=True), 0, [])
    for a, column in zip(arrays, columns):
        piece = filled[..., at : at + column.shape[along]]
        outs.append(piece.reshape(*piece.shape[:along], *a.shape[along:]))
        at += column.shape[along]
    return tuple(outs)


def side_by_side(arrays, axis, split_dim, concat_dim, along):
    both = jnp.concatenate(arrays, axis=along)
    filled, at, outs = (
        lax.all_to_all(both, axis, split_axis=split_dim, concat_axis=concat_dim, tiled=True),
        0,
        [],
    )
    for a in arrays:
        outs.append(lax.slice_in_dim(filled, at, at + a.shape[along], axis=along))
        at += a.shape[along]
    return tuple(outs)


def cut_along(x, dim, size):
    shape = x.shape
    pieces = x.reshape(*shape[:dim], size, shape[dim] // size, *shape[dim + 1 :])
    return jnp.moveaxis(pieces, dim, 0)


def sum_at_owner(x, axis, dim):
    pieces = cut_along(x, dim, lax.axis_size(axis))
    arrived = lax.all_to_all(pieces, axis, split_axis=0, concat_axis=0, tiled=True)
    return arrived.astype(jnp.float32).sum(axis=0)


def rms_rows(values, scales):
    values = values.astype(jnp.float32)
    return values * lax.rsqrt(jnp.mean(values * values, axis=-1, keepdims=True) + norm_eps) * scales


def rotary(values, position):
    middle = values.shape[-1] // 2
    inverse = rope_base ** (-jnp.arange(middle, dtype=jnp.float32) / middle)
    angles = position.astype(jnp.float32)[:, None] * inverse[None, :]
    cosine = jnp.cos(angles)[:, None, None, :]
    sine_part = jnp.sin(angles)[:, None, None, :]
    leading, second = (values[..., :middle], values[..., middle:])
    return jnp.concatenate(
        [leading * cosine - second * sine_part, second * cosine + leading * sine_part], axis=-1
    )


def per_device(
    hidden_in,
    past_lengths,
    key_cache,
    value_cache,
    attn_gain,
    w_query,
    w_key,
    w_value,
    lambdas,
    head_gain,
    w_out,
    ffn_gain,
    route_ids,
    route_weights,
    expert_gate,
    expert_up,
    expert_down,
    gate_vector,
    dense_gate,
    dense_up,
    dense_down,
):
    batch_rows = hidden_in.shape[0]
    model_width = hidden_in.shape[1]
    tp_count = lax.axis_size("tp")
    ep_count = lax.axis_size("ep")
    tp_rank = lax.axis_index("tp")
    half_width = model_width // tp_count
    heads_here = lambdas.shape[0]
    kv_here = w_key.shape[1] // (2 * HEAD_DIM)
    per_key = heads_here // kv_here
    scale_qk = HEAD_DIM ** (-0.5)
    normed = rms_rows(hidden_in, attn_gain).astype(jnp.bfloat16)
    queries = rotary(
        jnp.dot(normed, w_query, preferred_element_type=jnp.float32).reshape(
            batch_rows, heads_here, 2, HEAD_DIM
        ),
        past_lengths,
    ).astype(jnp.bfloat16)
    key_new = rotary(
        jnp.dot(normed, w_key, preferred_element_type=jnp.float32).reshape(
            batch_rows, kv_here, 2, HEAD_DIM
        ),
        past_lengths,
    ).astype(jnp.bfloat16)
    value_new = jnp.dot(normed, w_value, preferred_element_type=jnp.float32).astype(jnp.bfloat16)
    grouped = queries.reshape(batch_rows, kv_here, per_key, 2, HEAD_DIM)
    own_score = (
        jnp.einsum("sgamd,sgmd->sgam", grouped, key_new, preferred_element_type=jnp.float32)
        * scale_qk
    )
    value_rows = value_new.reshape(batch_rows, kv_here, 1, 1, VALUE_DIM).astype(jnp.float32)
    start_state = (
        own_score,
        jnp.ones_like(own_score),
        jnp.broadcast_to(value_rows, own_score.shape + (VALUE_DIM,)),
    )
    cache_len = key_cache.shape[1]
    span_len = min(256, cache_len)
    spans_needed = (jnp.max(past_lengths) + span_len - 1) // span_len

    def visit(block_index, carried):
        running, totals, summed = carried
        offset = block_index * span_len
        key_rows = lax.dynamic_slice_in_dim(key_cache, offset, span_len, 1).reshape(
            batch_rows, span_len, kv_here, 2, HEAD_DIM
        )
        cached = lax.dynamic_slice_in_dim(value_cache, offset, span_len, 1).reshape(
            batch_rows, span_len, kv_here, VALUE_DIM
        )
        scores = (
            jnp.einsum("sgamd,slgmd->sgaml", grouped, key_rows, preferred_element_type=jnp.float32)
            * scale_qk
        )
        usable = (offset + jnp.arange(span_len))[None, :] < past_lengths[:, None]
        scores = jnp.where(usable[:, None, None, None, :], scores, -jnp.inf)
        raised = jnp.maximum(running, jnp.max(scores, axis=-1))
        fading = jnp.exp(running - raised)
        weights = jnp.exp(scores - raised[..., None])
        totals = totals * fading + jnp.sum(weights, axis=-1)
        summed = summed * fading[..., None] + jnp.einsum(
            "sgaml,slge->sgame",
            weights.astype(jnp.bfloat16),
            cached,
            preferred_element_type=jnp.float32,
        )
        return (raised, totals, summed)

    running, totals, summed = lax.fori_loop(0, spans_needed, visit, start_state)
    mapped = summed / totals[..., None]
    head_mix = mapped[..., 0, :] - lambdas.reshape(1, kv_here, per_key, 1) * mapped[..., 1, :]
    head_out = rms_rows(head_mix, head_gain).astype(jnp.bfloat16).reshape(batch_rows, -1)
    attn_out = (
        taken_together(
            jnp.dot(head_out, w_out, preferred_element_type=jnp.float32).astype(jnp.bfloat16), "tp"
        )
        .astype(jnp.float32)
        .astype(jnp.bfloat16)
    )
    residual = hidden_in.astype(jnp.float32) + attn_out.astype(jnp.float32)
    moe_in = rms_rows(residual, ffn_gain).astype(jnp.bfloat16)
    mix_gate = jax.nn.sigmoid(
        jnp.dot(moe_in, gate_vector, preferred_element_type=jnp.float32)
    ).astype(jnp.bfloat16)
    top_count = route_ids.shape[1]
    experts = ep_count // 2
    capacity = max(2, 2 * batch_rows * top_count // experts)
    flat_ids = route_ids.reshape(-1)
    matches = (flat_ids[:, None] == jnp.arange(experts)[None, :]).astype(jnp.int32)
    earlier = jnp.sum((jnp.cumsum(matches, axis=0) - matches) * matches, axis=1)
    slot_of = flat_ids * capacity + earlier
    placing = (jnp.arange(experts * capacity)[:, None] == slot_of[None, :]).astype(jnp.float32)
    repeated = jnp.repeat(moe_in, top_count, axis=0)
    packed = jnp.dot(
        placing.astype(jnp.bfloat16), repeated, preferred_element_type=jnp.float32
    ).astype(jnp.bfloat16)
    outgoing = jnp.broadcast_to(
        packed.reshape(experts, 1, capacity, model_width), (experts, 2, capacity, model_width)
    ).reshape(ep_count, capacity, model_width)
    arrived = lax.all_to_all(outgoing, "ep", split_axis=0, concat_axis=0, tiled=True)
    leading = arrived.shape[:2]
    flat_rows = arrived.reshape(-1, model_width)
    gate_pre = jnp.dot(flat_rows, expert_gate[0], preferred_element_type=jnp.float32)
    up_pre = jnp.dot(flat_rows, expert_up[0], preferred_element_type=jnp.float32)
    inner_act = (jax.nn.silu(gate_pre) * up_pre).astype(jnp.bfloat16)
    inner_act = collect(inner_act, "tp", 1)
    partial_value = jnp.dot(inner_act, expert_down[0], preferred_element_type=jnp.float32).reshape(
        leading + (half_width,)
    )
    returned = lax.all_to_all(
        partial_value.astype(jnp.bfloat16), "ep", split_axis=0, concat_axis=0, tiled=True
    ).astype(partial_value.dtype)
    paired = jnp.sum(returned.reshape(experts, 2, capacity, half_width), axis=1).reshape(
        experts * capacity, half_width
    )
    weighted = (
        (placing * route_weights.reshape(1, -1))
        .reshape(experts * capacity, batch_rows, top_count)
        .sum(axis=2)
    )
    moe_out = jnp.einsum("ct,cd->td", weighted, paired, precision=lax.Precision.HIGHEST)
    own_half = lax.dynamic_slice_in_dim(moe_in, tp_rank * half_width, half_width, 1)
    rows_all, gates_all = in_one_piece((own_half, mix_gate), "ep", 0, 1)
    columns = dense_gate.shape[1]
    gate_cols, up_cols = side_by_side(
        (
            dense_gate.reshape(tp_count, half_width, columns),
            dense_up.reshape(tp_count, half_width, columns),
        ),
        "tp",
        0,
        2,
        1,
    )
    pre_gate, pre_up = (
        taken_together(
            jnp.dot(rows_all, gate_cols[0], preferred_element_type=jnp.float32).astype(
                jnp.bfloat16
            ),
            "tp",
        ).astype(jnp.float32),
        taken_together(
            jnp.dot(rows_all, up_cols[0], preferred_element_type=jnp.float32).astype(jnp.bfloat16),
            "tp",
        ).astype(jnp.float32),
    )
    dense_act = (jax.nn.silu(pre_gate) * pre_up).astype(jnp.bfloat16)
    gate_rows = gates_all.astype(jnp.float32)
    dense_out = sum_at_owner(
        (
            jnp.dot(dense_act, dense_down, preferred_element_type=jnp.float32) * gate_rows[:, None]
        ).astype(jnp.bfloat16),
        "ep",
        0,
    )
    own_residual = lax.dynamic_slice_in_dim(residual, tp_rank * half_width, half_width, 1)
    mixed_out = (own_residual + moe_out + dense_out).astype(jnp.bfloat16)
    return (mixed_out, key_new.reshape(batch_rows, -1), value_new)


def solution(mesh):
    return jax.shard_map(
        per_device,
        mesh=mesh,
        in_specs=(
            P("ep", None),
            P("ep"),
            P("ep", None, "tp"),
            P("ep", None, "tp"),
            P(),
            P(None, "tp"),
            P(None, "tp"),
            P(None, "tp"),
            P("tp"),
            P(),
            P("tp", None),
            P(),
            P("ep", None),
            P("ep", None),
            P("ep", None, "tp"),
            P("ep", None, "tp"),
            P("ep", None, "tp"),
            P(),
            P(None, ("ep", "tp")),
            P(None, ("ep", "tp")),
            P("ep", "tp"),
        ),
        out_specs=(P("ep", "tp"), P("ep", "tp"), P("ep", "tp")),
        check_vma=False,
    )
```

profile of v0, /device:TPU:0, one launch (start us, length us, event | category | flops | bytes accessed | tf_op | source)
XLA Modules:
  0.0 275.7 jit_solution(12817063429684109780)
XLA Ops:
  10.4 3.2 %fusion.73 = f32[32,1024]{1,0:T(8,128)S(1)} fusion(bf16[2048,1024]{1,0:T(8,128)(2,1)} %param.28, bf16[32,2048]{1,0:T(8,128)(2,1)} %param.23, f32[2048]{0:T(1024)} %param.27, f32[32]{0:T(128)S(1)} %add_rsqrt_fusion.2), kind=kOutput, calls=%fused_computation.116 | convolution fusion | flops 134479872 | bytes 4464768 | tf_op jit(solution)/shard_map/dot_general | solution.py:122
  18.3 57.8 %while.14 = (s32[]{:T(128)}, f32[32,1,8,2]{2,3,0,1:T(2,128)}, f32[32,1,8,2]{2,3,0,1:T(2,128)}, f32[32,1,8,2,128]{4,2,3,0,1:T(8,128)}, s32[]{:T(128)}, /*index=5*...) while((s32[]{:T(128)}, f32[32,1,8,2]{2,3,0,1:T(2,128)}, ...), condition=%wide.region_5.6_spmd, body=%wide.region_2.5_spmd.sunk | while | flops 51390212 | bytes 14797119 | solution.py:176
  18.3 3.1 %constant_dynamic-slice_fusion.3 = bf16[32,256,128]{2,1,0:T(8,128)(2,1)} fusion(bf16[32,1024,128]{2,1,0:T(8,128)(2,1)} %get-tuple-element.251, s32[]{:T(128)S(6)} %select_n.26), kind=kLoop, calls=%fused_computation.22.clone.1 | loop fusion | bytes 4194308 | tf_op jit(solution)/shard_map/while/body/dynamic_slice | solution.py:152
  21.4 3.3 %copy.152 = bf16[32,256,128]{1,2,0:T(8,128)(2,1)S(1)} copy(bf16[32,256,128]{2,1,0:T(8,128)(2,1)} %constant_dynamic-slice_fusion.3) | data formatting | bytes 4194304 | tf_op jit(solution)/shard_map/while/body/dynamic_slice | solution.py:152
  32.7 3.1 %constant_dynamic-slice_fusion.3 = bf16[32,256,128]{2,1,0:T(8,128)(2,1)} fusion(bf16[32,1024,128]{2,1,0:T(8,128)(2,1)} %get-tuple-element.251, s32[]{:T(128)S(6)} %select_n.26), kind=kLoop, calls=%fused_computation.22.clone.1 | loop fusion | bytes 4194308 | tf_op jit(solution)/shard_map/while/body/dynamic_slice | solution.py:152
  35.9 3.3 %copy.152 = bf16[32,256,128]{1,2,0:T(8,128)(2,1)S(1)} copy(bf16[32,256,128]{2,1,0:T(8,128)(2,1)} %constant_dynamic-slice_fusion.3) | data formatting | bytes 4194304 | tf_op jit(solution)/shard_map/while/body/dynamic_slice | solution.py:152
  47.2 3.1 %constant_dynamic-slice_fusion.3 = bf16[32,256,128]{2,1,0:T(8,128)(2,1)} fusion(bf16[32,1024,128]{2,1,0:T(8,128)(2,1)} %get-tuple-element.251, s32[]{:T(128)S(6)} %select_n.26), kind=kLoop, calls=%fused_computation.22.clone.1 | loop fusion | bytes 4194308 | tf_op jit(solution)/shard_map/while/body/dynamic_slice | solution.py:152
  50.3 3.3 %copy.152 = bf16[32,256,128]{1,2,0:T(8,128)(2,1)S(1)} copy(bf16[32,256,128]{2,1,0:T(8,128)(2,1)} %constant_dynamic-slice_fusion.3) | data formatting | bytes 4194304 | tf_op jit(solution)/shard_map/while/body/dynamic_slice | solution.py:152
  64.8 3.3 %copy.152 = bf16[32,256,128]{1,2,0:T(8,128)(2,1)S(1)} copy(bf16[32,256,128]{2,1,0:T(8,128)(2,1)} %constant_dynamic-slice_fusion.3) | data formatting | bytes 4194304 | tf_op jit(solution)/shard_map/while/body/dynamic_slice | solution.py:152
  82.8 3.4 %all-to-all-start = ((bf16[2,32,2048]{2,1,0:T(8,128)(2,1)}), bf16[2,32,2048]{2,1,0:T(8,128)(2,1)S(1)}, u32[]{:S(2)}, u32[]{:S(2)}) async-start(bf16[2,32,2048]{2,1,0:T(8,128)(2,1)} %broadcast_in_dim.37), calls=%async_computation | async-start | bytes 524288 | tf_op jit(solution)/shard_map/all_to_all | solution.py:16
  90.9 3.5 %all-to-all-start.4 = ((bf16[2,2048,44]{1,2,0:T(8,128)(2,1)}), bf16[2,2048,44]{1,2,0:T(8,128)(2,1)S(1)}, u32[]{:S(2)}, u32[]{:S(2)}) async-start(bf16[2,2048,44]{1,2,0:T(8,128)(2,1)} %pad_maximum_fusion), calls=%async_computation.4 | async-start | bytes 786432 | tf_op jit(solution)/shard_map/all_to_all | solution.py:48
  97.8 11.4 %all-to-all-start.1 = ((bf16[64,4,2048]{2,1,0:T(4,128)(2,1)}), bf16[64,4,2048]{2,1,0:T(4,128)(2,1)S(1)}, u32[]{:S(2)}, u32[]{:S(2)}) async-start(bf16[64,4,2048]{2,1,0:T(4,128)(2,1)} %bitcast.26), calls=%async_computation.1 | async-start | bytes 2097152 | tf_op jit(solution)/shard_map/all_to_all | solution.py:207
  110.0 18.8 %all-to-all-done.1 = bf16[64,4,2048]{2,1,0:T(4,128)(2,1)S(1)} async-done(((bf16[64,4,2048]{2,1,0:T(4,128)(2,1)}), bf16[64,4,2048]{2,1,0:T(4,128)(2,1)S(1)}, u32[]{:S(2)}, u32[]{:S(2)}) %all-to-all-start.1) | async-done | bytes 1048608 | tf_op jit(solution)/shard_map/all_to_all | solution.py:207
  133.0 4.1 %all_to_all.53 = bf16[2,256,352]{1,2,0:T(8,128)(2,1)S(1)} all-to-all(bf16[2,256,352]{1,2,0:T(8,128)(2,1)S(1)} %broadcast_in_dim.41), channel_id=1, replica_groups=mesh['ep'=64,'tp'=2] {'tp'}, dimensions={0} | all-to-all | bytes 720896 | tf_op jit(solution)/shard_map/all_to_all | solution.py:16
  139.9 28.0 %all-gather.2.cloned.1.call-done = bf16[2048,1025]{1,0:T(8,128)(2,1)} async-done(((bf16[32,1025]{1,0:T(8,128)(2,1)}), bf16[2048,1025]{1,0:T(8,128)(2,1)}) %all-gather.2.cloned.1.call-update) | async-done | bytes 4198416 | tf_op jit(solution)/shard_map/all_gather | solution.py:37
  167.8 3.6 %fusion.27 = bf16[2048,88]{0,1:T(8,128)(2,1)S(1)} fusion(bf16[2048,1025]{1,0:T(8,128)(2,1)} %all-gather.2.cloned.1.call-done, bf16[1,2048,88]{1,2,0:T(8,128)(2,1)S(1)} %copy-done.6), kind=kOutput, calls=%fused_computation.31 | convolution fusion | flops 369278976 | bytes 4734976 | tf_op jit(solution)/shard_map/dot_general | solution.py:250
  172.4 3.7 %all-to-all-start.6 = ((bf16[2,2048,88]{1,2,0:T(8,128)(2,1)}), bf16[2,2048,88]{1,2,0:T(8,128)(2,1)S(1)}, u32[]{:S(2)}, u32[]{:S(2)}) async-start(bf16[2,2048,88]{1,2,0:T(8,128)(2,1)} %broadcast_in_dim.43), calls=%async_computation.6 | async-start | bytes 1441792 | tf_op jit(solution)/shard_map/all_to_all | solution.py:16
  176.1 3.6 %fusion.24 = bf16[2048,88]{0,1:T(8,128)(2,1)S(1)} fusion(bf16[2048,1025]{1,0:T(8,128)(2,1)} %all-gather.2.cloned.1.call-done, bf16[1,2048,88]{1,2,0:T(8,128)(2,1)S(1)} %copy-done.6), kind=kOutput, calls=%fused_computation.30 | convolution fusion | flops 369278976 | bytes 4734976 | tf_op jit(solution)/shard_map/dot_general | solution.py:244
  180.7 3.5 %all-to-all-start.5 = ((bf16[2,2048,88]{1,2,0:T(8,128)(2,1)}), bf16[2,2048,88]{1,2,0:T(8,128)(2,1)S(1)}, u32[]{:S(2)}, u32[]{:S(2)}) async-start(bf16[2,2048,88]{1,2,0:T(8,128)(2,1)} %broadcast_in_dim.42), calls=%async_computation.5 | async-start | bytes 1441792 | tf_op jit(solution)/shard_map/all_to_all | solution.py:16
  186.1 6.5 %all-to-all-start.3 = ((bf16[64,4,1024]{2,1,0:T(4,128)(2,1)}), bf16[64,4,1024]{2,1,0:T(4,128)(2,1)S(1)}, u32[]{:S(2)}, u32[]{:S(2)}) async-start(bf16[64,4,1024]{2,1,0:T(4,128)(2,1)} %copy.120), calls=%async_computation.3 | async-start | bytes 1048576 | tf_op jit(solution)/shard_map/all_to_all | solution.py:217
  194.0 4.4 %multiply_convert_fusion = bf16[2048,1024]{1,0:T(8,128)(2,1)} fusion(bf16[88,1024]{1,0:T(8,128)(2,1)S(1)} %copy-done.20, f32[2048]{0:T(1024)S(1)} %convert_reduce_fusion.4, f32[2048,88]{0,1:T(8,128)} %convert_reduce_fusion.1, f32[2048,88]{0,1:T(8,128)S(1)} %convert_reduce_fusion.2), kind=kOutput, calls=%fused_computation.24 | convolution fusion | flops 374374400 | bytes 5824512 | tf_op jit(solution)/shard_map/dot_general | solution.py:258
  198.4 7.9 %all-to-all-done.3 = bf16[64,4,1024]{2,1,0:T(4,128)(2,1)S(1)} async-done(((bf16[64,4,1024]{2,1,0:T(4,128)(2,1)}), bf16[64,4,1024]{2,1,0:T(4,128)(2,1)S(1)}, u32[]{:S(2)}, u32[]{:S(2)}) %all-to-all-start.3) | async-done | bytes 524320 | tf_op jit(solution)/shard_map/all_to_all | solution.py:217
  206.3 5.8 %all-to-all-start.7 = ((bf16[64,32,1024]{2,1,0:T(8,128)(2,1)}), bf16[64,32,1024]{2,1,0:T(8,128)(2,1)}, u32[]{:S(2)}, u32[]{:S(2)}) async-start(bf16[64,32,1024]{2,1,0:T(8,128)(2,1)} %bitcast.180), calls=%async_computation.7 | async-start | bytes 8388608 | tf_op jit(solution)/shard_map/all_to_all | solution.py:66
  213.7 51.1 %all-to-all-done.7 = bf16[64,32,1024]{2,1,0:T(8,128)(2,1)} async-done(((bf16[64,32,1024]{2,1,0:T(8,128)(2,1)}), bf16[64,32,1024]{2,1,0:T(8,128)(2,1)}, u32[]{:S(2)}, u32[]{:S(2)}) %all-to-all-start.7) | async-done | bytes 4194336 | tf_op jit(solution)/shard_map/all_to_all | solution.py:66
  (156 shorter events, 75.4 us)
Async XLA Ops:
  7.2 130.9 %copy-start = (bf16[1,704,1024]{2,1,0:T(8,128)(2,1)S(1)}, bf16[1,704,1024]{2,1,0:T(8,128)(2,1)}, u32[]{:S(2)}) copy-start(bf16[1,704,1024]{2,1,0:T(8,128)(2,1)} %param.39) | copy-start | bytes 4325380
  7.2 6.9 %copy-start.1 = (bf16[32,2048]{1,0:T(8,128)(2,1)S(1)}, bf16[32,2048]{1,0:T(8,128)(2,1)}, u32[]{:S(2)}) copy-start(bf16[32,2048]{1,0:T(8,128)(2,1)} %param.23) | copy-start | bytes 393220
  7.2 6.9 %copy-start.11 = (f32[2048]{0:T(1024)S(1)}, f32[2048]{0:T(1024)}, u32[]{:S(2)}) copy-start(f32[2048]{0:T(1024)} %param.27) | copy-start | bytes 24580
  7.2 6.9 %copy-start.4 = (bf16[2048,128]{1,0:T(8,128)(2,1)S(1)}, bf16[2048,128]{1,0:T(8,128)(2,1)}, u32[]{:S(2)}) copy-start(bf16[2048,128]{1,0:T(8,128)(2,1)} %param.29) | copy-start | bytes 1572868
  7.2 8.7 %copy-start.5 = (bf16[2048,128]{1,0:T(8,128)(2,1)S(1)}, bf16[2048,128]{1,0:T(8,128)(2,1)}, u32[]{:S(2)}) copy-start(bf16[2048,128]{1,0:T(8,128)(2,1)} %param.30) | copy-start | bytes 1572868
  76.1 11.7 %copy-start.2 = (bf16[32,2048]{1,0:T(8,128)(2,1)S(1)}, bf16[32,2048]{1,0:T(8,128)(2,1)}, u32[]{:S(2)}) copy-start(bf16[32,2048]{1,0:T(8,128)(2,1)} %param.23) | copy-start | bytes 393220
  76.1 12.6 %copy-start.14 = (bf16[2048]{0:T(1024)(128)(2,1)S(1)}, bf16[2048]{0:T(1024)(128)(2,1)}, u32[]{:S(2)}) copy-start(bf16[2048]{0:T(1024)(128)(2,1)} %param.40) | copy-start | bytes 12292
  76.1 12.6 %copy-start.13 = (f32[2048]{0:T(1024)S(1)}, f32[2048]{0:T(1024)}, u32[]{:S(2)}) copy-start(f32[2048]{0:T(1024)} %param.34) | copy-start | bytes 24580
  77.3 12.5 %copy-start.7 = (bf16[2048,44]{0,1:T(8,128)(2,1)S(1)}, bf16[2048,44]{0,1:T(8,128)(2,1)}, u32[]{:S(2)}) copy-start(bf16[2048,44]{0,1:T(8,128)(2,1)} %param.42) | copy-start | bytes 540676
  79.0 11.0 %copy-start.8 = (bf16[2048,44]{0,1:T(8,128)(2,1)S(1)}, bf16[2048,44]{0,1:T(8,128)(2,1)}, u32[]{:S(2)}) copy-start(bf16[2048,44]{0,1:T(8,128)(2,1)} %param.41) | copy-start | bytes 540676
  79.1 15.3 %copy-start.15 = (s32[32,2]{0,1:T(2,128)S(1)}, s32[32,2]{0,1:T(2,128)}, u32[]{:S(2)}) copy-start(s32[32,2]{0,1:T(2,128)} %param.35) | copy-start | bytes 772
  82.8 5.0 %all-to-all-start = ((bf16[2,32,2048]{2,1,0:T(8,128)(2,1)}), bf16[2,32,2048]{2,1,0:T(8,128)(2,1)S(1)}, u32[]{:S(2)}, u32[]{:S(2)}) async-start(bf16[2,32,2048]{2,1,0:T(8,128)(2,1)} %broadcast_in_dim.37), calls=%async_computation | async-start | bytes 524288 | tf_op jit(solution)/shard_map/all_to_all | solution.py:16
  86.2 81.6 %all-gather.2.cloned.1.call-start = ((), (), s32[]{:S(2)}) async-start(), calls=%async_computation.8 | async-start | bytes 4792320 | tf_op jit(solution)/shard_map/all_gather | solution.py:37
  90.9 5.3 %all-to-all-start.4 = ((bf16[2,2048,44]{1,2,0:T(8,128)(2,1)}), bf16[2,2048,44]{1,2,0:T(8,128)(2,1)S(1)}, u32[]{:S(2)}, u32[]{:S(2)}) async-start(bf16[2,2048,44]{1,2,0:T(8,128)(2,1)} %pad_maximum_fusion), calls=%async_computation.4 | async-start | bytes 786432 | tf_op jit(solution)/shard_map/all_to_all | solution.py:48
  97.8 31.0 %all-to-all-start.1 = ((bf16[64,4,2048]{2,1,0:T(4,128)(2,1)}), bf16[64,4,2048]{2,1,0:T(4,128)(2,1)S(1)}, u32[]{:S(2)}, u32[]{:S(2)}) async-start(bf16[64,4,2048]{2,1,0:T(4,128)(2,1)} %bitcast.26), calls=%async_computation.1 | async-start | bytes 2097152 | tf_op jit(solution)/shard_map/all_to_all | solution.py:207
  133.0 34.8 %copy-start.6 = (bf16[1,2048,88]{1,2,0:T(8,128)(2,1)S(1)}, bf16[1,2048,88]{1,2,0:T(8,128)(2,1)}, u32[]{:S(2)}) copy-start(bf16[1,2048,88]{1,2,0:T(8,128)(2,1)} %all_to_all.41) | copy-start | bytes 1081348
  172.4 7.3 %all-to-all-start.6 = ((bf16[2,2048,88]{1,2,0:T(8,128)(2,1)}), bf16[2,2048,88]{1,2,0:T(8,128)(2,1)S(1)}, u32[]{:S(2)}, u32[]{:S(2)}) async-start(bf16[2,2048,88]{1,2,0:T(8,128)(2,1)} %broadcast_in_dim.43), calls=%async_computation.6 | async-start | bytes 1441792 | tf_op jit(solution)/shard_map/all_to_all | solution.py:16
  179.7 14.3 %copy-start.20 = (bf16[88,1024]{1,0:T(8,128)(2,1)S(1)}, bf16[88,1024]{1,0:T(8,128)(2,1)}, u32[]{:S(2)}) copy-start(bf16[88,1024]{1,0:T(8,128)(2,1)} %param.43) | copy-start | bytes 540676
  180.7 5.4 %all-to-all-start.5 = ((bf16[2,2048,88]{1,2,0:T(8,128)(2,1)}), bf16[2,2048,88]{1,2,0:T(8,128)(2,1)S(1)}, u32[]{:S(2)}, u32[]{:S(2)}) async-start(bf16[2,2048,88]{1,2,0:T(8,128)(2,1)} %broadcast_in_dim.42), calls=%async_computation.5 | async-start | bytes 1441792 | tf_op jit(solution)/shard_map/all_to_all | solution.py:16
  186.1 20.1 %all-to-all-start.3 = ((bf16[64,4,1024]{2,1,0:T(4,128)(2,1)}), bf16[64,4,1024]{2,1,0:T(4,128)(2,1)S(1)}, u32[]{:S(2)}, u32[]{:S(2)}) async-start(bf16[64,4,1024]{2,1,0:T(4,128)(2,1)} %copy.120), calls=%async_computation.3 | async-start | bytes 1048576 | tf_op jit(solution)/shard_map/all_to_all | solution.py:217
  206.3 6.8 %copy-start.16 = (s32[32,2]{0,1:T(2,128)S(1)}, s32[32,2]{0,1:T(2,128)}, u32[]{:S(2)}) copy-start(s32[32,2]{0,1:T(2,128)} %param.35) | copy-start | bytes 772
  206.3 6.8 %copy-start.19 = (f32[32,2]{0,1:T(2,128)S(1)}, f32[32,2]{0,1:T(2,128)}, u32[]{:S(2)}) copy-start(f32[32,2]{0,1:T(2,128)} %param.36) | copy-start | bytes 772
  206.3 58.5 %all-to-all-start.7 = ((bf16[64,32,1024]{2,1,0:T(8,128)(2,1)}), bf16[64,32,1024]{2,1,0:T(8,128)(2,1)}, u32[]{:S(2)}, u32[]{:S(2)}) async-start(bf16[64,32,1024]{2,1,0:T(8,128)(2,1)} %bitcast.180), calls=%async_computation.7 | async-start | bytes 8388608 | tf_op jit(solution)/shard_map/all_to_all | solution.py:66
  212.1 55.7 %copy-start.3 = (f32[32,2048]{1,0:T(8,128)S(1)}, f32[32,2048]{1,0:T(8,128)}, u32[]{:S(2)}) copy-start(f32[32,2048]{1,0:T(8,128)} %get-tuple-element.141) | copy-start | bytes 786436
  (5 other events, 18.0 us)
Sparse Core Ops, SparseCore 0:
  89.9 77.8 all-gather.1
where the time goes:
time: 278 us; the launch traced here: 276 us
  waiting for transfers between devices  108 us (39%)
  local copies, waits for them, and re-layouts  41.1 us (15%)
  matrix products  41.1 us (15%)
  starting transfers between devices  37.8 us (14%)
  other arithmetic  28 us (10%)
  between operations  15.3 us (6%)
  blocking collectives  4.14 us (1%)
    all_to_all x1, waiting for transfers between devices, sum_at_owner(): lax.all_to_all(pieces, axis, split_axis=0, concat_axis=0, tiled=True)  51.1 us
    all_gather x1, waiting for transfers between devices, in_one_piece(): filled, at, outs = (lax.all_gather(both, axis, axis=dim, tiled=True), 0, [])  28 us
    dynamic_slice x8, local copies, waits for them, and re-layouts, visit(): lax.dynamic_slice_in_dim(key_cache, offset, span_len, 1)  25.7 us
    all_to_all x1, waiting for transfers between devices, per_device(): lax.all_to_all(outgoing, 'ep', split_axis=0, concat_axis=0, tiled=True)  18.8 us
    all_to_all x1, starting transfers between devices, per_device(): lax.all_to_all(outgoing, 'ep', split_axis=0, concat_axis=0, tiled=True)  11.4 us
    dot_general x4, matrix products, visit(): jnp.einsum('sgaml,slge->sgame', weights.astype(jnp.bfloat16), cached, pre...  11.1 us
    all_to_all x3, starting transfers between devices, sent_to_all(): lax.all_to_all(jnp.broadcast_to(x[None], (size, *x.shape)), axis, 0, 0, t...  10.7 us
    all_to_all x1, waiting for transfers between devices, per_device(): lax.all_to_all(partial_value.astype(jnp.bfloat16), 'ep', split_axis=0, co...  7.86 us
  transfers between devices with their start and end apart: 8, of which 6 were waited for; matrix products, arithmetic and copies ran while one was open for 8% of the time, Pallas kernels for 0%

commit v1 on v0

v1 whole, which is shorter than its diff:
```python
import functools

import jax
import jax.numpy as jnp
from jax import lax
from jax.experimental import pallas as pl
from jax.experimental.pallas import tpu as pltpu
from jax.sharding import PartitionSpec as P

EPS = 1e-05
ROPE_BASE = 10000.0
BF = jnp.bfloat16
F32 = jnp.float32
ROWS = 32
WIDTH = 2048
HALF = 1024
CACHE = 1024
GRP = 4
NGRP = ROWS // GRP
NT = (((1,), (1,)), ((), ()))
TN = (((0,), (0,)), ((), ()))


def dot(a, b):
    return jnp.dot(a, b, preferred_element_type=F32)


def dot_nt(a, b):
    return lax.dot_general(a, b, NT, preferred_element_type=F32)


def dot_tn(a, b):
    return lax.dot_general(a, b, TN, preferred_element_type=F32)


def layer_kernel(
    hid, trig, plen, again, lam, hgain, fgain, route,
    kc_h, vc_h, wq_h, wk_h, wv_h, wo_h, eg_h, eu_h, ed_h, wd_h, dd_h,
    out, nk, nv,
    kb, vb, wq, wk, wv, wo, eg, eu, ed,
    wdg, ddg, qs, kn, vn, ho, pbuf, resid, rt, G, D, X, abuf, Y, R,
    dact, gsc, sel, selw, pb, s1, tb, s2,
    lsem, kvsem, wdss, wdrs, ddss, ddrs, tps, tpr, rts, rtr,
    gss, grs, gds, gdr, zs, zr, xds, xdr, as_, ar, das, dar, ys, yr,
    r1s, r1r, r2s, r2r,
):
    c = lax.axis_index("tp")
    ep = lax.axis_index("ep")
    z = ep // 16
    p0 = ep % 16
    y = p0 // 4
    x = p0 % 4
    sa = 1 + 3 * c
    sb = 4 - 3 * c
    a = x * (1 - c) + y * c
    b = y * (1 - c) + x * c
    zb = z * 16
    half = pl.ds(pl.multiple_of(c * HALF, HALF), HALF)
    other = 1 - c

    def local(src, dst, sem):
        return pltpu.make_async_copy(src, dst, sem)

    def remote(src, dst, ssem, rsem, **dev):
        return pltpu.make_async_remote_copy(
            src_ref=src, dst_ref=dst, send_sem=ssem, recv_sem=rsem,
            device_id=dev, device_id_type=pl.DeviceIdType.MESH,
        )

    def pidx(aa, bb):
        return aa * sa + bb * sb

    first = [
        local(wq_h, wq, lsem.at[0]),
        local(wk_h, wk, lsem.at[1]),
        local(wv_h, wv, lsem.at[2]),
    ]
    for cp in first:
        cp.start()

    def kv(g):
        rows = pl.ds(g * GRP, GRP)
        return (
            local(kc_h.at[rows], kb.at[rows], kvsem.at[0, g]),
            local(vc_h.at[rows], vb.at[rows], kvsem.at[1, g]),
        )

    own_w = local(wd_h, wdg.at[:, z], lsem.at[3])
    own_d = local(dd_h, ddg.at[:, z], lsem.at[4])
    own_w.start()
    own_d.start()

    @pl.loop(0, NGRP)
    def _(g):
        for cp in kv(g):
            cp.start()

    later = [
        local(wo_h, wo, lsem.at[5]),
        local(eg_h.at[0], eg, lsem.at[6]),
        local(eu_h.at[0], eu, lsem.at[7]),
        local(ed_h.at[0], ed, lsem.at[8]),
    ]
    for cp in later:
        cp.start()

    barrier = pltpu.get_barrier_semaphore()
    for k in range(1, 16):
        dest = zb + ((y + k // 4) % 4) * 4 + (x + k % 4) % 4
        pl.semaphore_signal(barrier, inc=1, device_id={"ep": dest}, device_id_type=pl.DeviceIdType.MESH)
    for k in range(1, 4):
        dest = ((z + k) % 4) * 16 + p0
        pl.semaphore_signal(barrier, inc=1, device_id={"ep": dest}, device_id_type=pl.DeviceIdType.MESH)
    pl.semaphore_signal(barrier, inc=1, device_id={"tp": other}, device_id_type=pl.DeviceIdType.MESH)
    pl.semaphore_wait(barrier, 19)

    def rt_copy(k):
        dest = zb + ((y + k // 4) % 4) * 4 + (x + k % 4) % 4
        return remote(route, rt.at[p0], rts.at[k], rtr.at[k], ep=dest)

    for k in range(1, 16):
        rt_copy(k).start()
    rt[p0] = route[...]

    own_w.wait()
    own_d.wait()

    def w_copy(k):
        dest = ((z + k) % 4) * 16 + p0
        return (
            remote(wdg.at[:, z], wdg.at[:, z], wdss.at[k], wdrs.at[k], ep=dest),
            remote(ddg.at[:, z], ddg.at[:, z], ddss.at[k], ddrs.at[k], ep=dest),
        )

    for k in (1, 3, 2):
        for cp in w_copy(k):
            cp.start()

    h = hid[...].astype(F32)
    normed = (h * lax.rsqrt(jnp.mean(h * h, axis=-1, keepdims=True) + EPS) * again[...]).astype(BF)
    cos = trig[0]
    sin = trig[1]
    low = (lax.broadcasted_iota(jnp.int32, (ROWS, 128), 1) & 63) < 32

    def rotated(v):
        turned = jnp.where(low, pltpu.roll(v, 96, 1), pltpu.roll(v, 32, 1))
        return (v * cos + turned * sin).astype(BF)

    for cp in first:
        cp.wait()
    new_k = rotated(dot(normed, wk[...]))
    new_v = dot(normed, wv[...]).astype(BF)
    nk[...] = new_k
    nv[...] = new_v
    kn[...] = new_k.astype(F32)
    vn[...] = new_v.astype(F32)
    q = dot(normed, wq[...])
    for i in range(8):
        qs[:, i, :] = rotated(q[:, i * 128 : (i + 1) * 128]).astype(F32) * 0.125

    lam_col = jnp.zeros((8, 128), F32)
    rows8 = lax.broadcasted_iota(jnp.int32, (8, 128), 0)
    for i in range(8):
        lam_col = jnp.where(rows8 == i, lam[i], lam_col)
    left = lax.broadcasted_iota(jnp.int32, (8, 128), 1) < 64
    last16 = lax.broadcasted_iota(jnp.int32, (16, 128), 0) == 15
    places = lax.broadcasted_iota(jnp.int32, (16, CACHE), 1)
    gain = hgain[...]

    @pl.loop(0, NGRP)
    def _(g):
        for cp in kv(g):
            cp.wait()
        for i in range(GRP):
            s = g * GRP + i
            tail = pl.ds(CACHE - 16, 16)
            kb[s, tail, :] = jnp.where(
                last16, jnp.broadcast_to(kn[pl.ds(s, 1), :], (16, 128)), kb[s, tail, :].astype(F32)
            ).astype(BF)
            vb[s, tail, :] = jnp.where(
                last16, jnp.broadcast_to(vn[pl.ds(s, 1), :], (16, 128)), vb[s, tail, :].astype(F32)
            ).astype(BF)
            qv = qs[s]
            q2 = jnp.concatenate(
                [jnp.where(left, qv, 0.0), jnp.where(left, 0.0, qv)], axis=0
            ).astype(BF)
            scores = dot_nt(q2, kb[s])
            usable = (places < plen[s]) | (places == CACHE - 1)
            scores = jnp.where(usable, scores, -jnp.inf)
            peak = jnp.max(scores, axis=-1, keepdims=True)
            weights = jnp.exp(scores - peak)
            total = jnp.sum(weights, axis=-1, keepdims=True)
            mapped = dot(weights.astype(BF), vb[s]) / total
            mix = mapped[0:8] - lam_col * mapped[8:16]
            ho[s] = mix * lax.rsqrt(jnp.mean(mix * mix, axis=-1, keepdims=True) + EPS) * gain

    later[0].wait()
    head_out = jnp.concatenate([ho[:, i, :].astype(BF) for i in range(8)], axis=1)
    pbuf[0] = dot(head_out, wo[...]).astype(BF)
    tp_copy = remote(pbuf.at[0], pbuf.at[1], tps, tpr, tp=other)
    tp_copy.start()
    tp_copy.wait()
    attn_out = (pbuf[0].astype(F32) + pbuf[1].astype(F32)).astype(BF)
    res = hid[...].astype(F32) + attn_out.astype(F32)
    resid[...] = res
    G[p0] = (
        res * lax.rsqrt(jnp.mean(res * res, axis=-1, keepdims=True) + EPS) * fgain[...]
    ).astype(BF)

    def g_copy(ka, kb_, da, db):
        src = pidx((a + 4 - ka) % 4, (b + 4 - kb_) % 4)
        dest = zb + pidx((a + da) % 4, (b + db) % 4)
        i = (ka + da) * 4 + kb_ + db
        return remote(
            G.at[src, :, half], G.at[src, :, half], gss.at[i], grs.at[i], ep=dest
        )

    def g_wait(ka, kb_):
        i = ka * 4 + kb_
        src = pidx((a + 4 - ka) % 4, (b + 4 - kb_) % 4)
        remote(
            G.at[src, :, half], G.at[src, :, half], gss.at[i], grs.at[i], tp=other
        ).wait_recv()

    def g_share(ka, kb_):
        src = pidx((a + 4 - ka) % 4, (b + 4 - kb_) % 4)
        i = ka * sa + kb_ * sb
        return remote(
            G.at[src, :, half], G.at[src, :, half], gds.at[i], gdr.at[i], tp=other
        )

    for k in (1, 3, 2):
        g_copy(0, 0, k, 0).start()
        g_copy(0, 0, 0, k).start()
    for k in range(1, 16):
        src = ((y + 4 - k // 4) % 4) * 4 + (x + 4 - k % 4) % 4
        remote(route, rt.at[src], rts.at[k], rtr.at[k], tp=other).wait_recv()
    facts = jnp.concatenate(
        [rt[4 * i] + rt[4 * i + 1] + rt[4 * i + 2] + rt[4 * i + 3] for i in range(4)], axis=1
    )
    row = lax.broadcasted_iota(jnp.int32, (256, 512), 0)
    token = lax.broadcasted_iota(jnp.int32, (256, 512), 1)
    target = ((((row >> 6) * 16 + p0) >> 1) * 4 + (row & 3)).astype(F32)
    mine = ((row >> 2) & 15) == (token >> 5)
    hit0 = mine & (facts[0:1] == target)
    hit1 = mine & (facts[1:2] == target)
    sel[...] = jnp.where(hit0 | hit1, 1.0, 0.0).astype(BF)
    selw[...] = (jnp.where(hit0, facts[2:3], 0.0) + jnp.where(hit1, facts[3:4], 0.0)).astype(BF)

    for ka in (1, 3, 2):
        g_wait(ka, 0)
        for k in (1, 3, 2):
            g_copy(ka, 0, 0, k).start()
        g_share(ka, 0).start()
    for ka in (0, 1, 3, 2):
        for kb_ in (1, 3, 2):
            g_wait(ka, kb_)
            g_share(ka, kb_).start()

    D[...] = dot(sel[...], G[:, :, half].reshape(512, HALF)).astype(BF).reshape(4, 64, HALF)

    def z_copy(k):
        to = (z + k) % 4
        return remote(D.at[to], X.at[z, :, half], zs.at[k], zr.at[k], ep=to * 16 + p0)

    def x_share(k):
        src = (z + 4 - k) % 4
        return remote(X.at[src, :, half], X.at[src, :, half], xds.at[k], xdr.at[k], tp=other)

    for k in (1, 3, 2):
        z_copy(k).start()
    X[z, :, half] = D[z]
    x_share(0).start()

    for k in range(1, 16):
        src = ((y + 4 - k // 4) % 4) * 4 + (x + 4 - k % 4) % 4
        oh = pl.ds(pl.multiple_of(other * HALF, HALF), HALF)
        remote(G.at[src, :, oh], G.at[src, :, oh], gds.at[k], gdr.at[k], tp=other).wait_recv()
    for k in range(1, 4):
        src = (z + 4 - k) % 4
        remote(wdg.at[:, src], wdg.at[:, src], wdss.at[k], wdrs.at[k], tp=other).wait_recv()
        remote(ddg.at[:, src], ddg.at[:, src], ddss.at[k], ddrs.at[k], tp=other).wait_recv()

    @pl.loop(0, 4)
    def _(i):
        tokens = G[pl.ds(i * 4, 4)].reshape(128, WIDTH)
        pre_gate = dot_nt(tokens, wdg[0].reshape(192, WIDTH))
        pre_up = dot_nt(tokens, wdg[1].reshape(192, WIDTH))
        act = pre_gate / (1.0 + jnp.exp(-pre_gate)) * pre_up
        dact[c, pl.ds(i * 128, 128), :] = jnp.concatenate(
            [act, jnp.zeros((128, 64), F32)], axis=1
        ).astype(BF)
        mix_gate = (1.0 / (1.0 + jnp.exp(-pre_gate[:, 44:45]))).astype(BF).astype(F32)
        gsc[pl.ds(i * 128, 128), :] = jnp.broadcast_to(mix_gate, (128, 128))

    act_copy = remote(dact.at[c], dact.at[c], das, dar, tp=other)
    act_copy.start()

    for k in (1, 3, 2):
        src = (z + 4 - k) % 4
        remote(D.at[0], X.at[src, :, half], zs.at[k], zr.at[k], tp=other).wait_recv()
        x_share(k).start()
    for cp in later[1:]:
        cp.wait()
    for k in (0, 1, 3, 2):
        src = (z + 4 - k) % 4
        oh = pl.ds(pl.multiple_of(other * HALF, HALF), HALF)
        remote(X.at[src, :, oh], X.at[src, :, oh], xds.at[k], xdr.at[k], tp=other).wait_recv()
    rows_in = X[...].reshape(256, WIDTH)
    gate_pre = dot(rows_in, eg[...])
    up_pre = dot(rows_in, eu[...])
    inner = gate_pre / (1.0 + jnp.exp(-gate_pre)) * up_pre
    abuf[c] = jnp.concatenate([inner, jnp.zeros((256, 32), F32)], axis=1).astype(BF)
    a_copy = remote(abuf.at[c], abuf.at[c], as_, ar, tp=other)
    a_copy.start()
    remote(abuf.at[other], abuf.at[other], as_, ar, tp=other).wait_recv()
    Y[...] = (
        dot(abuf[0][:, :352], ed[0:352, :]) + dot(abuf[1][:, :352], ed[352:704, :])
    ).astype(BF).reshape(4, 64, HALF)

    def y_copy(k):
        to = (z + k) % 4
        return remote(Y.at[to], R.at[z], ys.at[k], yr.at[k], ep=to * 16 + p0)

    for k in (1, 3, 2):
        y_copy(k).start()
    R[z] = Y[z]
    remote(dact.at[other], dact.at[other], das, dar, tp=other).wait_recv()
    for k in (1, 3, 2):
        src = (z + 4 - k) % 4
        remote(Y.at[0], R.at[src], ys.at[k], yr.at[k], tp=other).wait_recv()

    @pl.loop(0, 4)
    def _(i):
        rows = pl.ds(pl.multiple_of(i * 128, 128), 128)
        part = dot(dact[0, rows, :][:, :192], ddg[0].reshape(192, HALF)) + dot(
            dact[1, rows, :][:, :192], ddg[1].reshape(192, HALF)
        )
        part = part * gsc[rows, 0:1] + dot_tn(selw[:, rows], R[...].reshape(256, HALF))
        part = part.astype(BF).reshape(4, ROWS, HALF)
        for j in range(4):
            pb[i * sb + j * sa] = part[j]

    def r1_copy(k):
        to = (b + k) % 4
        return remote(
            pb.at[pl.ds(to * 4, 4)], s1.at[k - 1], r1s.at[k], r1r.at[k], ep=zb + pidx(a, to)
        )

    def r2_copy(k):
        to = (a + k) % 4
        return remote(tb.at[to], s2.at[k - 1], r2s.at[k], r2r.at[k], ep=zb + pidx(to, b))

    for k in (1, 3, 2):
        r1_copy(k).start()
    for k in (1, 3, 2):
        r1_copy(k).wait_recv()
    total1 = pb[pl.ds(b * 4, 4)].astype(F32)
    for k in range(3):
        total1 = total1 + s1[k].astype(F32)
    tb[...] = total1.astype(BF)
    for k in (1, 3, 2):
        r2_copy(k).start()
    for k in (1, 3, 2):
        r2_copy(k).wait_recv()
    final = tb[a].astype(F32)
    for k in range(3):
        final = final + s2[k].astype(F32)
    out[...] = (resid[:, half] + final).astype(BF)

    for k in range(1, 16):
        rt_copy(k).wait_send()
    for k in range(1, 4):
        for cp in w_copy(k):
            cp.wait_send()
        g_copy(0, 0, k, 0).wait_send()
        g_copy(0, 0, 0, k).wait_send()
        z_copy(k).wait_send()
        y_copy(k).wait_send()
        r1_copy(k).wait_send()
        r2_copy(k).wait_send()
    for ka in range(1, 4):
        for k in range(1, 4):
            g_copy(ka, 0, 0, k).wait_send()
    for ka in range(4):
        for kb_ in range(4):
            if ka or kb_:
                g_share(ka, kb_).wait_send()
    for k in range(4):
        x_share(k).wait_send()
    act_copy.wait_send()
    a_copy.wait_send()


def routing_block(route_ids, route_weights, x):
    same = route_ids[:, :, None, None] == route_ids[None, None, :, :]
    at = jnp.arange(ROWS)
    before = (at[None, :] < at[:, None])[:, None, :, None]
    rank = jnp.sum((same & before).astype(F32), axis=(2, 3))
    code = route_ids.astype(F32) * 4.0 + rank
    vals = jnp.concatenate([code, route_weights], axis=1)
    vals = jnp.concatenate([vals, jnp.zeros_like(vals)], axis=1)
    place = jnp.arange(128)[None, :] == (at + 32 * x)[:, None]
    return jnp.sum(jnp.where(place[:, None, :], vals[:, :, None], 0.0), axis=0)


def per_device(
    hidden_in, past_lengths, key_cache, value_cache, attn_gain, w_query, w_key, w_value,
    lambdas, head_gain, w_out, ffn_gain, route_ids, route_weights, expert_gate, expert_up,
    expert_down, gate_vector, dense_gate, dense_up, dense_down,
):
    lane = jnp.arange(128)
    inverse = ROPE_BASE ** (-(lane % 32).astype(F32) / 32)
    angles = past_lengths.astype(F32)[:, None] * inverse[None, :]
    sign = jnp.where(lane % 64 < 32, -1.0, 1.0)
    trig = jnp.stack([jnp.cos(angles), jnp.sin(angles) * sign])
    route = routing_block(route_ids, route_weights, lax.axis_index("ep") % 4)
    wd = jnp.stack(
        [
            jnp.concatenate([dense_gate.T, gate_vector[None], jnp.zeros((3, WIDTH), BF)]),
            jnp.concatenate([dense_up.T, jnp.zeros((4, WIDTH), BF)]),
        ]
    )
    dd = jnp.pad(dense_down.reshape(2, 44, HALF), ((0, 0), (0, 4), (0, 0)))
    vm = pl.BlockSpec(memory_space=pltpu.VMEM)
    sm = pl.BlockSpec(memory_space=pltpu.SMEM)
    hbm = pl.BlockSpec(memory_space=pl.ANY)
    V = pltpu.VMEM
    dma = pltpu.SemaphoreType.DMA
    scratch = [
        V((ROWS, CACHE, 128), BF), V((ROWS, CACHE, 128), BF),
        V((WIDTH, 1024), BF), V((WIDTH, 128), BF), V((WIDTH, 128), BF), V((1024, WIDTH), BF),
        V((WIDTH, 352), BF), V((WIDTH, 352), BF), V((704, HALF), BF),
        V((2, 4, 48, WIDTH), BF), V((2, 4, 48, HALF), BF),
        V((ROWS, 8, 128), F32), V((ROWS, 128), F32), V((ROWS, 128), F32), V((ROWS, 8, 128), F32),
        V((2, ROWS, WIDTH), BF), V((ROWS, WIDTH), F32), V((16, 8, 128), F32),
        V((16, ROWS, WIDTH), BF), V((4, 64, HALF), BF), V((4, 64, WIDTH), BF),
        V((2, 256, 384), BF), V((4, 64, HALF), BF), V((4, 64, HALF), BF),
        V((2, 512, 256), BF), V((512, 128), F32), V((256, 512), BF), V((256, 512), BF),
        V((16, ROWS, HALF), BF), V((3, 4, ROWS, HALF), BF), V((4, ROWS, HALF), BF),
        V((3, ROWS, HALF), BF),
        dma((9,)), dma((2, NGRP)), dma((4,)), dma((4,)), dma((4,)), dma((4,)), dma, dma,
        dma((16,)), dma((16,)),
        dma((16,)), dma((16,)), dma((16,)), dma((16,)), dma((4,)), dma((4,)), dma((4,)), dma((4,)),
        dma, dma, dma, dma, dma((4,)), dma((4,)),
        dma((4,)), dma((4,)), dma((4,)), dma((4,)),
    ]
    return pl.pallas_call(
        layer_kernel,
        name="layer",
        out_shape=(
            jax.ShapeDtypeStruct((ROWS, HALF), BF),
            jax.ShapeDtypeStruct((ROWS, 128), BF),
            jax.ShapeDtypeStruct((ROWS, 128), BF),
        ),
        in_specs=[vm, vm, sm, vm, sm, vm, vm, vm] + [hbm] * 11,
        out_specs=(vm, vm, vm),
        scratch_shapes=scratch,
        compiler_params=pltpu.CompilerParams(
            collective_id=0, has_side_effects=True, vmem_limit_bytes=66 * 1000 * 1000
        ),
    )(
        hidden_in, trig, past_lengths, attn_gain.reshape(1, WIDTH), lambdas,
        head_gain.reshape(1, 128), ffn_gain.reshape(1, WIDTH), route,
        key_cache, value_cache, w_query, w_key, w_value, w_out, expert_gate, expert_up,
        expert_down, wd, dd,
    )


def solution(mesh):
    return jax.shard_map(
        per_device,
        mesh=mesh,
        in_specs=(
            P("ep", None), P("ep"), P("ep", None, "tp"), P("ep", None, "tp"), P(),
            P(None, "tp"), P(None, "tp"), P(None, "tp"), P("tp"), P(), P("tp", None), P(),
            P("ep", None), P("ep", None), P("ep", None, "tp"), P("ep", None, "tp"),
            P("ep", None, "tp"), P(), P(None, ("ep", "tp")), P(None, ("ep", "tp")), P("ep", "tp"),
        ),
        out_specs=(P("ep", "tp"), P("ep", "tp"), P("ep", "tp")),
        check_vma=False,
    )
```

time: 278 us -> 88.4 us (0.32)
  waiting for transfers between devices: 108 us -> 0 us
  Pallas kernels: 0 us -> 71 us
  matrix products: 41.1 us -> 0 us
  starting transfers between devices: 37.8 us -> 0 us
  local copies, waits for them, and re-layouts: 41.1 us -> 9.8 us
  other arithmetic: 28 us -> 6.58 us
  between operations: 15.3 us -> 0.69 us
  blocking collectives: 4.14 us -> 0 us
    all_to_all x7 -> x0, waiting for transfers between devices: 80.1 us -> none  [the longest x1 51.1 us: sum_at_owner(): lax.all_to_all(pieces, axis, split_axis=0, concat_axis=0, tiled=True)]
    pallas_call x0 -> x1, Pallas kernels: none -> 71 us  [per_device(): pl.pallas_call(layer_kernel, name='layer', out_shape=(jax.ShapeDtypeStruc...]
    dot_general x22 -> x0, matrix products: 41.1 us -> none  [the longest x4 11.1 us: visit(): jnp.einsum('sgaml,slge->sgame', weights.astype(jnp.bfloat16), cached, pre...]
    all_to_all x7 -> x0, starting transfers between devices: 37.8 us -> none  [the longest x1 11.4 us: per_device(): lax.all_to_all(outgoing, 'ep', split_axis=0, concat_axis=0, tiled=True)]
    all_gather x1 -> x0, waiting for transfers between devices: 28 us -> none  [in_one_piece(): filled, at, outs = (lax.all_gather(both, axis, axis=dim, tiled=True), 0, [])]
    dynamic_slice x9 -> x0, local copies, waits for them, and re-layouts: 25.7 us -> none  [the longest x8 25.7 us: visit(): lax.dynamic_slice_in_dim(key_cache, offset, span_len, 1)]
    unnamed x44 -> x9, local copies, waits for them, and re-layouts: 0.71 us -> 7.21 us
    reduce_sum x13 -> x2, other arithmetic: 7.78 us -> 1.61 us  [the longest x1 0.92 us: routing_block(): rank = jnp.sum((same & before).astype(F32), axis=(2, 3))]
  transfers between devices with their start and end apart: 8 -> 0, of which waited for: 6 -> 0; matrix products, arithmetic and copies ran while one was open for 8% -> 0% of each run, Pallas kernels for 0% -> 0%
where the time goes in v1:
time: 88.4 us; the launch traced here: 88 us
  Pallas kernels  71 us (80%)
  local copies, waits for them, and re-layouts  9.8 us (11%)
  other arithmetic  6.58 us (7%)
    pallas_call x1, Pallas kernels, per_device(): pl.pallas_call(layer_kernel, name='layer', out_shape=(jax.ShapeDtypeStruc...  71 us
    unnamed x9, local copies, waits for them, and re-layouts  7.21 us
    another operation x2, other arithmetic, per_device(): jnp.stack([jnp.concatenate([dense_gate.T, gate_vector[None], jnp.zeros((3...  1.91 us

profile of v1, /device:TPU:0, one launch (start us, length us, event | category | flops | bytes accessed | tf_op | source)
XLA Modules:
  0.0 88.0 jit_solution(9734438632206600028)
XLA Ops:
  0.6 0.0 copy-start
  0.7 0.8 convert_element_type.18
  1.4 0.1 pad.13.clone
  1.5 0.1 pad.10.clone
  1.6 0.1 iota_compare_fusion.1
  1.7 0.9 %convert_reduce_fusion = f32[32,2]{0,1:T(2,128)S(1)} fusion(s32[32,2]{0,1:T(2,128)} %param.33, pred[32,32]{1,0:T(8,128)(4,1)S(1)} %iota_compare_fusion), kind=kLoop, calls=%fused_computation.4 | loop fusion | flops 16320 | bytes 1536 | tf_op jit(solution)/shard_map/reduce_sum | solution.py:399
  2.6 0.7 multiply_add_fusion
  3.3 0.7 maximum_maximum_fusion
  4.0 0.7 broadcast_in_dim.56
  4.7 0.1 copy.41
  4.8 0.7 select_reduce_fusion.route
  5.5 0.1 multiply_cosine_fusion
  5.7 0.6 pad_maximum_fusion.1.trig
  6.3 1.0 %reshape.190 = bf16[2,44,1024]{2,1,0:T(8,128)(2,1)S(1)} reshape(bf16[88,1024]{1,0:T(8,128)(2,1)} %param.41) | data formatting | bytes 360448 | tf_op jit(solution)/shard_map/reshape | solution.py:424
  7.2 0.7 pad.5.dd_h
  7.9 1.1 %maximum_bitcast_fusion = (bf16[1,48,2048]{2,1,0:T(8,128)(2,1)S(1)}, bf16[1,48,2048]{2,1,0:T(8,128)(2,1)S(1)}) fusion(bf16[1,2048]{1,0:T(2,128)(2,1)S(1)} %broadcast_in_dim.56, bf16[44,2048]{1,0:T(8,128)(2,1)} %bitcast.9, bf16[48]{0:T(256)(128)(2,1)S(1)} %pad.10.clone, bf16[44,2048]{1,0:T(8,128)(2,1)} %bitcast.10), kind=kLoop, calls=%fused_computation.1 | loop fusion | flops 589824 | bytes 757856 | tf_op jit(solution)/shard_map/stack | solution.py:418
  9.1 0.8 pad_maximum_fusion.wd_h
  9.9 1.6 %copy.42.eg_h = bf16[1,2048,352]{2,1,0:T(8,128)(2,1)} copy(bf16[1,2048,352]{1,2,0:T(8,128)(2,1)S(1)} %copy-done) | data formatting | bytes 2883584 | tf_op args[14]
  11.4 0.0 copy-done.1
  11.4 1.6 %copy.43.eu_h = bf16[1,2048,352]{2,1,0:T(8,128)(2,1)} copy(bf16[1,2048,352]{1,2,0:T(8,128)(2,1)S(1)} %copy-done.1) | data formatting | bytes 2883584 | tf_op args[15]
  13.0 71.0 %layer.1 = (bf16[32,1024]{1,0:T(8,128)(2,1)}, bf16[32,128]{1,0:T(8,128)(2,1)}, bf16[32,128]{1,0:T(8,128)(2,1)}) custom-call(bf16[32,2048]{1,0:T(8,128)(2,1)} %hid.1, f32[2,32,128]{2,1,0:T(8,128)} %pad_maximum_fusion.1.trig, s32[32]{0:T(128)} %plen.1, f32[1,2048]{1,0:T(1,128)} %bitcast.11, f32[8]{0:T(128)} %lam.1, f32[1,128]{1,0:T(1,128)} %bitcast.13, ...), custom_call_target="tpu_custom_call" | custom-call | tf_op jit(solution)/shard_map/layer/pallas_call | solution.py:448
  84.0 1.5 %copy.47 = bf16[32,1024]{1,0:T(8,128)(2,1)} copy(bf16[32,1024]{1,0:T(8,128)(2,1)} %get-tuple-element.12) | data formatting | bytes 131072
  85.5 1.3 %copy.48 = bf16[32,128]{1,0:T(8,128)(2,1)} copy(bf16[32,128]{1,0:T(8,128)(2,1)} %get-tuple-element.13) | data formatting | bytes 16384
  86.7 1.3 %copy.49 = bf16[32,128]{1,0:T(8,128)(2,1)} copy(bf16[32,128]{1,0:T(8,128)(2,1)} %get-tuple-element.14) | data formatting | bytes 16384
  (7 shorter events, 0.0 us)
Async XLA Ops:
  0.6 9.2 %copy-start = (bf16[1,2048,352]{1,2,0:T(8,128)(2,1)S(1)}, bf16[1,2048,352]{1,2,0:T(8,128)(2,1)}, u32[]{:S(2)}) copy-start(bf16[1,2048,352]{1,2,0:T(8,128)(2,1)} %param.35) | copy-start | bytes 4325380
  9.9 1.6 %copy-start.1 = (bf16[1,2048,352]{1,2,0:T(8,128)(2,1)S(1)}, bf16[1,2048,352]{1,2,0:T(8,128)(2,1)}, u32[]{:S(2)}) copy-start(bf16[1,2048,352]{1,2,0:T(8,128)(2,1)} %param.36) | copy-start | bytes 4325380

commit v2 on v1

v2 whole, which is shorter than its diff:
```python
import jax
import jax.numpy as jnp
import numpy as np
from jax import lax
from jax.experimental import pallas as pl
from jax.experimental.pallas import tpu as pltpu
from jax.sharding import PartitionSpec as P

EPS = 1e-05
ROPE_BASE = 10000.0
BF = jnp.bfloat16
F32 = jnp.float32
ROWS = 32
WIDTH = 2048
HALF = 1024
CACHE = 1024
GRP = 4
NGRP = ROWS // GRP
NT = (((1,), (1,)), ((), ()))
TN = (((0,), (0,)), ((), ()))


def dot(a, b):
    return jnp.dot(a, b, preferred_element_type=F32)


def dot_nt(a, b):
    return lax.dot_general(a, b, NT, preferred_element_type=F32)


def dot_tn(a, b):
    return lax.dot_general(a, b, TN, preferred_element_type=F32)


def layer_kernel(
    hid, freq, plen, prow, again, lam, hgain, fgain, ids, wts, gvec,
    kc_h, vc_h, wq_h, wk_h, wv_h, wo_h, eg_h, eu_h, ed_h, dg_h, du_h, dd_h,
    out,
    kb, vb, wq, wk, wv, wo, eg, eu, ed, dg, du, dtail,
    wdg, ddg, qs, kn, vn, ho, pbuf, resid, rt, G, D, X, tz, abuf, Y, R, ty,
    dact, gsc, sel, selw, pb, s1, t1, m1, tb, s2, t2, m2,
    lsem, kvsem, wss, wrs, tps, tpr, rts, rtr,
    gss, grs, gds, gdr, zs, zr, xds, xdr, as_, ar, das, dar, ys, yr,
    r1s, r1r, r2s, r2r,
):
    c = lax.axis_index("tp")
    ep = lax.axis_index("ep")
    z = ep // 16
    p0 = ep % 16
    y = p0 // 4
    x = p0 % 4
    sa = 1 + 3 * c
    sb = 4 - 3 * c
    a = x * (1 - c) + y * c
    b = y * (1 - c) + x * c
    zb = z * 16
    other = 1 - c
    half = pl.ds(pl.multiple_of(c * HALF, HALF), HALF)
    other_half = pl.ds(pl.multiple_of(other * HALF, HALF), HALF)

    def local(src, dst, sem):
        return pltpu.make_async_copy(src, dst, sem)

    def remote(src, dst, ssem, rsem, **dev):
        return pltpu.make_async_remote_copy(
            src_ref=src, dst_ref=dst, send_sem=ssem, recv_sem=rsem,
            device_id=dev, device_id_type=pl.DeviceIdType.MESH,
        )

    def pidx(aa, bb):
        return aa * sa + bb * sb

    def z_ep(step):
        return ((z + 4 + step) % 4) * 16 + p0

    def a_ep(step):
        return zb + pidx((a + 4 + step) % 4, b)

    def b_ep(step):
        return zb + pidx(a, (b + 4 + step) % 4)

    own_w = [
        local(dg_h, dg, lsem.at[3]),
        local(du_h, du, lsem.at[4]),
        local(dd_h.at[pl.ds(0, 48)], ddg.at[0, z], lsem.at[9]),
        local(dd_h.at[pl.ds(40, 48)], dtail, lsem.at[10]),
    ]
    first = [
        local(wk_h, wk, lsem.at[1]),
        local(wv_h, wv, lsem.at[2]),
        local(wq_h, wq, lsem.at[0]),
    ]
    for cp in own_w + first:
        cp.start()

    def kv(g):
        rows = pl.ds(g * GRP, GRP)
        return (
            local(kc_h.at[rows], kb.at[rows], kvsem.at[0, g]),
            local(vc_h.at[rows], vb.at[rows], kvsem.at[1, g]),
        )

    @pl.loop(0, NGRP)
    def _(g):
        for cp in kv(g):
            cp.start()

    later = [
        local(wo_h, wo, lsem.at[5]),
        local(eg_h.at[0], eg, lsem.at[6]),
        local(eu_h.at[0], eu, lsem.at[7]),
        local(ed_h.at[0], ed, lsem.at[8]),
    ]
    for cp in later:
        cp.start()

    barrier = pltpu.get_barrier_semaphore()
    for k in range(1, 16):
        dest = zb + ((y + k // 4) % 4) * 4 + (x + k % 4) % 4
        pl.semaphore_signal(barrier, inc=1, device_id={"ep": dest}, device_id_type=pl.DeviceIdType.MESH)
    for step in (1, -1):
        pl.semaphore_signal(barrier, inc=1, device_id={"ep": z_ep(step)}, device_id_type=pl.DeviceIdType.MESH)
    pl.semaphore_signal(barrier, inc=1, device_id={"tp": other}, device_id_type=pl.DeviceIdType.MESH)

    for cp in own_w:
        cp.wait()
    gv = gvec[...].astype(F32)
    gv = jnp.concatenate([gv[i : i + 1] for i in range(16)], axis=1)
    pad_row = lax.broadcasted_iota(jnp.int32, (4, WIDTH), 0)
    wdg[0, z, 0:44, :] = dg[...]
    wdg[0, z, 44:48, :] = jnp.where(pad_row == 0, gv, 0.0).astype(BF)
    wdg[1, z, 0:44, :] = du[...]
    wdg[1, z, 44:48, :] = jnp.zeros((4, WIDTH), BF)
    ddg[1, z] = pltpu.roll(dtail[...].astype(F32), 44, 0).astype(BF)

    at = lax.broadcasted_iota(jnp.int32, (ROWS, 128), 0)
    lane = lax.broadcasted_iota(jnp.int32, (ROWS, 128), 1)
    diag = at == lane
    shifted = at + 32 * x == lane

    def lanes(v, fill):
        return jnp.concatenate([v.astype(F32), jnp.full((v.shape[0], 128 - ROWS), fill, F32)], axis=1)

    def column(v):
        return jnp.sum(jnp.where(diag, v, 0.0), axis=1, keepdims=True)

    def moved(col):
        return jnp.sum(jnp.where(shifted, col, 0.0), axis=0, keepdims=True)

    id_rows = lanes(ids[...], -1.0)
    wt_rows = lanes(wts[...], 0.0)
    earlier = lane < at
    facts = []
    for k in range(2):
        col = column(id_rows[k : k + 1])
        same = jnp.where(id_rows[0:1] == col, 1.0, 0.0) + jnp.where(id_rows[1:2] == col, 1.0, 0.0)
        rank = jnp.sum(jnp.where(earlier, same, 0.0), axis=1, keepdims=True)
        facts.append(moved(col * 4.0 + rank))
    for k in range(2):
        facts.append(moved(column(wt_rows[k : k + 1])))
    facts.append(jnp.zeros((4, 128), F32))
    rt[p0] = jnp.concatenate(facts, axis=0)

    pl.semaphore_wait(barrier, 18)

    def rt_copy(k):
        dest = zb + ((y + k // 4) % 4) * 4 + (x + k % 4) % 4
        return remote(rt.at[p0], rt.at[p0], rts.at[k], rtr.at[k], ep=dest)

    for k in range(1, 16):
        rt_copy(k).start()

    def w_copy(i):
        block = (z + 4 + (0, 0, 0, 0, -1, 1, -1, 1)[i]) % 4
        ref = (
            wdg.at[:, block], wdg.at[:, block], ddg.at[:, block], ddg.at[:, block],
            wdg.at[0, block], wdg.at[1, block], ddg.at[0, block], ddg.at[1, block],
        )[i]
        return remote(ref, ref, wss.at[i], wrs.at[i], ep=z_ep((1, -1)[i % 2]))

    def w_wait(i):
        block = (z + 4 + (-1, 1, -1, 1, -2, 2, -2, 2)[i]) % 4
        ref = (
            wdg.at[:, block], wdg.at[:, block], ddg.at[:, block], ddg.at[:, block],
            wdg.at[0, block], wdg.at[1, block], ddg.at[0, block], ddg.at[1, block],
        )[i]
        remote(ref, ref, wss.at[i], wrs.at[i], tp=other).wait_recv()

    for i in range(4):
        w_copy(i).start()

    h = hid[...].astype(F32)
    normed = (h * lax.rsqrt(jnp.mean(h * h, axis=-1, keepdims=True) + EPS) * again[...]).astype(BF)
    angles = column(lanes(prow[...], 0.0)) * freq[...]
    cos = jnp.cos(angles)
    low = (lane & 63) < 32
    sin = jnp.sin(angles) * jnp.where(low, -1.0, 1.0)

    def rotated(v):
        turned = jnp.where(low, pltpu.roll(v, 96, 1), pltpu.roll(v, 32, 1))
        return (v * cos + turned * sin).astype(BF)

    for cp in first:
        cp.wait()
    new_k = rotated(dot(normed, wk[...]))
    new_v = dot(normed, wv[...]).astype(BF)
    out[:, HALF : HALF + 128] = new_k
    out[:, HALF + 128 : HALF + 256] = new_v
    kn[...] = new_k.astype(F32)
    vn[...] = new_v.astype(F32)
    q = dot(normed, wq[...])
    for i in range(8):
        qs[:, i, :] = rotated(q[:, i * 128 : (i + 1) * 128]).astype(F32) * 0.125

    lam_col = jnp.zeros((8, 128), F32)
    rows8 = lax.broadcasted_iota(jnp.int32, (8, 128), 0)
    for i in range(8):
        lam_col = jnp.where(rows8 == i, lam[i], lam_col)
    left = lax.broadcasted_iota(jnp.int32, (8, 128), 1) < 64
    last16 = lax.broadcasted_iota(jnp.int32, (16, 128), 0) == 15
    places = lax.broadcasted_iota(jnp.int32, (16, CACHE), 1)
    gain = hgain[...]

    def attend(lo, hi):
        @pl.loop(lo, hi)
        def _(g):
            for cp in kv(g):
                cp.wait()
            for i in range(GRP):
                s = g * GRP + i
                tail = pl.ds(CACHE - 16, 16)
                kb[s, tail, :] = jnp.where(
                    last16, jnp.broadcast_to(kn[pl.ds(s, 1), :], (16, 128)), kb[s, tail, :].astype(F32)
                ).astype(BF)
                vb[s, tail, :] = jnp.where(
                    last16, jnp.broadcast_to(vn[pl.ds(s, 1), :], (16, 128)), vb[s, tail, :].astype(F32)
                ).astype(BF)
                qv = qs[s]
                q2 = jnp.concatenate(
                    [jnp.where(left, qv, 0.0), jnp.where(left, 0.0, qv)], axis=0
                ).astype(BF)
                scores = dot_nt(q2, kb[s])
                usable = (places < plen[s]) | (places == CACHE - 1)
                scores = jnp.where(usable, scores, -jnp.inf)
                peak = jnp.max(scores, axis=-1, keepdims=True)
                weights = jnp.exp(scores - peak)
                total = jnp.sum(weights, axis=-1, keepdims=True)
                mapped = dot(weights.astype(BF), vb[s]) / total
                mix = mapped[0:8] - lam_col * mapped[8:16]
                ho[s] = mix * lax.rsqrt(jnp.mean(mix * mix, axis=-1, keepdims=True) + EPS) * gain

    attend(0, NGRP)

    later[0].wait()
    head_out = jnp.concatenate([ho[:, i, :].astype(BF) for i in range(8)], axis=1)
    pbuf[0] = dot(head_out, wo[...]).astype(BF)
    tp_copy = remote(pbuf.at[0], pbuf.at[1], tps, tpr, tp=other)
    tp_copy.start()
    for i in range(4):
        w_wait(i)
        w_copy(4 + i).start()
    tp_copy.wait()
    attn_out = (pbuf[0].astype(F32) + pbuf[1].astype(F32)).astype(BF)
    res = hid[...].astype(F32) + attn_out.astype(F32)
    resid[...] = res
    G[p0] = (
        res * lax.rsqrt(jnp.mean(res * res, axis=-1, keepdims=True) + EPS) * fgain[...]
    ).astype(BF)

    JA = (0, -1, 1, 2)

    def g_block(ja, jb, rows=pl.ds(0, ROWS)):
        return G.at[pidx((a + 4 + ja) % 4, (b + 4 + jb) % 4), rows, half]

    lo16, hi16 = pl.ds(0, 16), pl.ds(16, 16)

    def g_copy(i):
        if i < 4:
            ref = (g_block(0, 0), g_block(0, 0), g_block(-1, 0, lo16), g_block(1, 0, hi16))[i]
            return remote(ref, ref, gss.at[i], grs.at[i], ep=a_ep((1, -1)[i % 2]))
        ja, k = JA[i // 4 - 1], i % 4
        ref = (g_block(ja, 0), g_block(ja, 0), g_block(ja, -1, lo16), g_block(ja, 1, hi16))[k]
        return remote(ref, ref, gss.at[i], grs.at[i], ep=b_ep((1, -1)[k % 2]))

    def g_wait(i):
        k = i % 4
        step, rows = ((-1, None), (1, None), (-2, lo16), (2, hi16))[k]
        rows = pl.ds(0, ROWS) if rows is None else rows
        ref = g_block(step, 0, rows) if i < 4 else g_block(JA[i // 4 - 1], step, rows)
        remote(ref, ref, gss.at[i], grs.at[i], tp=other).wait_recv()

    def g_share(ja, jb):
        i = ((4 - ja) % 4) * sa + ((4 - jb) % 4) * sb
        ref = g_block(ja, jb)
        return remote(ref, ref, gds.at[i], gdr.at[i], tp=other)

    for i in (0, 1, 4, 5):
        g_copy(i).start()

    for k in range(1, 16):
        src = ((y + 4 - k // 4) % 4) * 4 + (x + 4 - k % 4) % 4
        remote(rt.at[src], rt.at[src], rts.at[k], rtr.at[k], tp=other).wait_recv()
    facts = jnp.concatenate(
        [rt[4 * i] + rt[4 * i + 1] + rt[4 * i + 2] + rt[4 * i + 3] for i in range(4)], axis=1
    )
    row = lax.broadcasted_iota(jnp.int32, (256, 512), 0)
    token = lax.broadcasted_iota(jnp.int32, (256, 512), 1)
    target = ((((row >> 6) * 16 + p0) >> 1) * 4 + (row & 3)).astype(F32)
    mine = ((row >> 2) & 15) == (token >> 5)
    hit0 = mine & (facts[0:1] == target)
    hit1 = mine & (facts[1:2] == target)
    sel[...] = jnp.where(hit0 | hit1, 1.0, 0.0).astype(BF)
    selw[...] = (jnp.where(hit0, facts[2:3], 0.0) + jnp.where(hit1, facts[3:4], 0.0)).astype(BF)

    def b_first(j):
        for k in (0, 1):
            g_wait(4 + 4 * j + k)
            g_copy(6 + 4 * j + k).start()
            g_share(JA[j], (-1, 1)[k]).start()

    def b_last(j):
        g_wait(6 + 4 * j)
        g_wait(7 + 4 * j)
        g_share(JA[j], 2).start()

    for k in (0, 1):
        g_wait(k)
        g_copy(2 + k).start()
        g_copy(8 + 4 * k).start()
        g_copy(9 + 4 * k).start()
        g_share((-1, 1)[k], 0).start()
    b_first(0)
    g_wait(2)
    g_wait(3)
    g_copy(16).start()
    g_copy(17).start()
    g_share(2, 0).start()
    b_first(1)
    b_last(0)
    b_first(2)
    b_last(1)
    b_first(3)
    b_last(2)
    b_last(3)

    D[...] = dot(sel[...], G[:, :, half].reshape(512, HALF)).astype(BF).reshape(4, 64, HALF)
    lo32, hi32 = pl.ds(0, 32), pl.ds(32, 32)
    whole = pl.ds(0, 64)

    def x_at(step, rows=whole):
        return X.at[(z + 4 + step) % 4, rows, half]

    def r_at(step, rows=whole):
        return R.at[(z + 4 + step) % 4, rows]

    def ring_copy(i, src, at_, mid, ss, rs):
        def piece(step, rows=whole):
            return src.at[(z + 4 + step) % 4, rows]

        pairs = (
            (piece(2, lo32), mid.at[0]), (piece(2, hi32), mid.at[1]),
            (piece(1), at_(0)), (piece(-1), at_(0)),
            (mid.at[0], at_(-1, lo32)), (mid.at[1], at_(1, hi32)),
        )
        return remote(pairs[i][0], pairs[i][1], ss.at[i], rs.at[i], ep=z_ep((1, -1)[i % 2]))

    def ring_wait(i, at_, mid, ss, rs):
        ref = (mid.at[0], mid.at[1], at_(-1), at_(1), at_(-2, lo32), at_(2, hi32))[i]
        remote(ref, ref, ss.at[i], rs.at[i], tp=other).wait_recv()

    def z_copy(i):
        return ring_copy(i, D, x_at, tz, zs, zr)

    def z_wait(i):
        ring_wait(i, x_at, tz, zs, zr)

    def x_share(step):
        i = (4 - step) % 4
        ref = x_at(step)
        return remote(ref, ref, xds.at[i], xdr.at[i], tp=other)

    for i in range(4):
        z_copy(i).start()
    X[z, :, half] = D[z]
    x_share(0).start()

    for i in range(4, 8):
        w_wait(i)
    for k in range(1, 16):
        src = ((y + 4 - k // 4) % 4) * 4 + (x + 4 - k % 4) % 4
        ref = G.at[src, :, other_half]
        remote(ref, ref, gds.at[k], gdr.at[k], tp=other).wait_recv()

    def dense_rows(i):
        tokens = G[pl.ds(i * 4, 4)].reshape(128, WIDTH)
        pre_gate = dot_nt(tokens, wdg[0].reshape(192, WIDTH))
        pre_up = dot_nt(tokens, wdg[1].reshape(192, WIDTH))
        act = pre_gate / (1.0 + jnp.exp(-pre_gate)) * pre_up
        rows = pl.ds(pl.multiple_of(i * 128, 128), 128)
        dact[c, rows, :] = jnp.concatenate([act, jnp.zeros((128, 64), F32)], axis=1).astype(BF)
        mix_gate = (1.0 / (1.0 + jnp.exp(-pre_gate[:, 44:45]))).astype(BF).astype(F32)
        gsc[rows, :] = jnp.broadcast_to(mix_gate, (128, 128))

    for i in (0, 1):
        z_wait(i)
        z_copy(4 + i).start()
    for i in (2, 3):
        z_wait(i)
        x_share((-1, 1)[i - 2]).start()

    @pl.loop(0, 4)
    def _(i):
        dense_rows(i)

    act_copy = remote(dact.at[c], dact.at[c], das, dar, tp=other)
    act_copy.start()

    z_wait(4)
    z_wait(5)
    x_share(2).start()
    for cp in later[1:]:
        cp.wait()
    for step in (0, -1, 1, 2):
        ref = X.at[(z + 4 + step) % 4, :, other_half]
        i = (4 - step) % 4
        remote(ref, ref, xds.at[i], xdr.at[i], tp=other).wait_recv()
    rows_in = X[...].reshape(256, WIDTH)
    gate_pre = dot_nt(rows_in, eg[...])
    up_pre = dot_nt(rows_in, eu[...])
    inner = gate_pre / (1.0 + jnp.exp(-gate_pre)) * up_pre
    abuf[c] = jnp.concatenate([inner, jnp.zeros((256, 32), F32)], axis=1).astype(BF)
    a_copy = remote(abuf.at[c], abuf.at[c], as_, ar, tp=other)
    a_copy.start()
    remote(abuf.at[other], abuf.at[other], as_, ar, tp=other).wait_recv()
    Y[...] = (
        dot(abuf[0][:, :352], ed[0:352, :]) + dot(abuf[1][:, :352], ed[352:704, :])
    ).astype(BF).reshape(4, 64, HALF)

    def y_copy(i):
        return ring_copy(i, Y, r_at, ty, ys, yr)

    def y_wait(i):
        ring_wait(i, r_at, ty, ys, yr)

    for i in range(4):
        y_copy(i).start()
    R[z] = Y[z]
    for i in (0, 1):
        y_wait(i)
        y_copy(4 + i).start()
    remote(dact.at[other], dact.at[other], das, dar, tp=other).wait_recv()
    for i in (2, 3, 4, 5):
        y_wait(i)

    @pl.loop(0, 4)
    def _(i):
        rows = pl.ds(pl.multiple_of(i * 128, 128), 128)
        part = dot(dact[0, rows, :][:, :192], ddg[0].reshape(192, HALF)) + dot(
            dact[1, rows, :][:, :192], ddg[1].reshape(192, HALF)
        )
        part = part * gsc[rows, 0:1] + dot_tn(selw[:, rows], R[...].reshape(256, HALF))
        part = part.astype(BF).reshape(4, ROWS, HALF)
        for j in range(4):
            pb[i * sb + j * sa] = part[j]

    def sum_ring(block, arrive, passing, merged, dest, ss, rs, n):
        upper, lower = pl.ds(0, n), pl.ds(n, n)

        def copy(i):
            pairs = (
                (block(2, upper), passing.at[0]), (block(2, lower), passing.at[1]),
                (block(1, lower), arrive.at[0, lower]), (block(-1, upper), arrive.at[1, upper]),
                (merged.at[0], arrive.at[0, upper]), (merged.at[1], arrive.at[1, lower]),
            )
            return remote(pairs[i][0], pairs[i][1], ss.at[i], rs.at[i], ep=dest((1, -1)[i % 2]))

        def wait(i):
            ref = (
                passing.at[0], passing.at[1], arrive.at[0, lower], arrive.at[1, upper],
                arrive.at[0, upper], arrive.at[1, lower],
            )[i]
            remote(ref, ref, ss.at[i], rs.at[i], tp=other).wait_recv()

        for i in range(4):
            copy(i).start()
        for i in (0, 1):
            wait(i)
            mine_ = block((1, -1)[i], (upper, lower)[i])
            merged[i] = (mine_[...].astype(F32) + passing[i].astype(F32)).astype(BF)
            copy(4 + i).start()
        for i in range(2, 6):
            wait(i)
        return copy

    def b_block(step, part):
        return pb.at[pl.ds(((b + 4 + step) % 4) * 4 + part.start, part.size)]

    def a_block(step, part):
        return tb.at[(a + 4 + step) % 4, part]

    r1_copy = sum_ring(b_block, s1, t1, m1, b_ep, r1s, r1r, 2)
    tb[...] = (
        pb[pl.ds(b * 4, 4)].astype(F32) + s1[0].astype(F32) + s1[1].astype(F32)
    ).astype(BF)
    r2_copy = sum_ring(a_block, s2, t2, m2, a_ep, r2s, r2r, 16)
    out[:, :HALF] = (
        resid[:, half] + (tb[a].astype(F32) + s2[0].astype(F32) + s2[1].astype(F32))
    ).astype(BF)

    for k in range(1, 16):
        rt_copy(k).wait_send()
    for i in range(8):
        w_copy(i).wait_send()
    for i in range(20):
        g_copy(i).wait_send()
    for i in range(6):
        z_copy(i).wait_send()
        y_copy(i).wait_send()
        r1_copy(i).wait_send()
        r2_copy(i).wait_send()
    for ja in JA:
        for jb in JA:
            if ja or jb:
                g_share(ja, jb).wait_send()
    for step in JA:
        x_share(step).wait_send()
    act_copy.wait_send()
    a_copy.wait_send()


def split_kernel(both, out, nk, nv, sem):
    copies = [
        pltpu.make_async_copy(both.at[:, pl.ds(0, HALF)], out, sem.at[0]),
        pltpu.make_async_copy(both.at[:, pl.ds(HALF, 128)], nk, sem.at[1]),
        pltpu.make_async_copy(both.at[:, pl.ds(HALF + 128, 128)], nv, sem.at[2]),
    ]
    for cp in copies:
        cp.start()
    for cp in copies:
        cp.wait()


def per_device(
    hidden_in, past_lengths, key_cache, value_cache, attn_gain, w_query, w_key, w_value,
    lambdas, head_gain, w_out, ffn_gain, route_ids, route_weights, expert_gate, expert_up,
    expert_down, gate_vector, dense_gate, dense_up, dense_down,
):
    freq = np.power(np.float32(ROPE_BASE), -(np.arange(128) % 32).astype(np.float32) / np.float32(32))
    freq = jnp.asarray(freq.astype(np.float32)[None])
    vm = pl.BlockSpec(memory_space=pltpu.VMEM)
    sm = pl.BlockSpec(memory_space=pltpu.SMEM)
    hbm = pl.BlockSpec(memory_space=pl.ANY)
    V = pltpu.VMEM
    dma = pltpu.SemaphoreType.DMA
    scratch = [
        V((ROWS, CACHE, 128), BF), V((ROWS, CACHE, 128), BF),
        V((WIDTH, 1024), BF), V((WIDTH, 128), BF), V((WIDTH, 128), BF), V((1024, WIDTH), BF),
        V((352, WIDTH), BF), V((352, WIDTH), BF), V((704, HALF), BF),
        V((44, WIDTH), BF), V((44, WIDTH), BF), V((48, HALF), BF),
        V((2, 4, 48, WIDTH), BF), V((2, 4, 48, HALF), BF),
        V((ROWS, 8, 128), F32), V((ROWS, 128), F32), V((ROWS, 128), F32), V((ROWS, 8, 128), F32),
        V((2, ROWS, WIDTH), BF), V((ROWS, WIDTH), F32), V((16, 8, 128), F32),
        V((16, ROWS, WIDTH), BF), V((4, 64, HALF), BF), V((4, 64, WIDTH), BF), V((2, 32, HALF), BF),
        V((2, 256, 384), BF), V((4, 64, HALF), BF), V((4, 64, HALF), BF), V((2, 32, HALF), BF),
        V((2, 512, 256), BF), V((512, 128), F32), V((256, 512), BF), V((256, 512), BF),
        V((16, ROWS, HALF), BF), V((2, 4, ROWS, HALF), BF), V((2, 2, ROWS, HALF), BF),
        V((2, 2, ROWS, HALF), BF), V((4, ROWS, HALF), BF),
        V((2, ROWS, HALF), BF), V((2, 16, HALF), BF), V((2, 16, HALF), BF),
        dma((11,)), dma((2, NGRP)), dma((8,)), dma((8,)), dma, dma,
        dma((16,)), dma((16,)),
        dma((20,)), dma((20,)), dma((16,)), dma((16,)), dma((6,)), dma((6,)), dma((4,)), dma((4,)),
        dma, dma, dma, dma, dma((6,)), dma((6,)),
        dma((6,)), dma((6,)), dma((6,)), dma((6,)),
    ]
    both = pl.pallas_call(
        layer_kernel,
        name="layer",
        out_shape=jax.ShapeDtypeStruct((ROWS, HALF + 256), BF),
        in_specs=[vm, vm, sm, vm, vm, sm, vm, vm, vm, vm, vm] + [hbm] * 12,
        out_specs=vm,
        scratch_shapes=scratch,
        compiler_params=pltpu.CompilerParams(
            collective_id=0, has_side_effects=True, vmem_limit_bytes=66 * 1000 * 1000
        ),
    )(
        hidden_in, freq, past_lengths, past_lengths.reshape(1, ROWS), attn_gain.reshape(1, WIDTH),
        lambdas, head_gain.reshape(1, 128), ffn_gain.reshape(1, WIDTH), route_ids.T,
        route_weights.T, gate_vector.reshape(16, 128),
        key_cache, value_cache, w_query, w_key, w_value, w_out,
        expert_gate.swapaxes(1, 2), expert_up.swapaxes(1, 2), expert_down,
        dense_gate.T, dense_up.T, dense_down,
    )
    return pl.pallas_call(
        split_kernel,
        name="split",
        out_shape=(
            jax.ShapeDtypeStruct((ROWS, HALF), BF),
            jax.ShapeDtypeStruct((ROWS, 128), BF),
            jax.ShapeDtypeStruct((ROWS, 128), BF),
        ),
        in_specs=[hbm],
        out_specs=(hbm, hbm, hbm),
        scratch_shapes=[dma((3,))],
    )(both)


def solution(mesh):
    return jax.shard_map(
        per_device,
        mesh=mesh,
        in_specs=(
            P("ep", None), P("ep"), P("ep", None, "tp"), P("ep", None, "tp"), P(),
            P(None, "tp"), P(None, "tp"), P(None, "tp"), P("tp"), P(), P("tp", None), P(),
            P("ep", None), P("ep", None), P("ep", None, "tp"), P("ep", None, "tp"),
            P("ep", None, "tp"), P(), P(None, ("ep", "tp")), P(None, ("ep", "tp")), P("ep", "tp"),
        ),
        out_specs=(P("ep", "tp"), P("ep", "tp"), P("ep", "tp")),
        check_vma=False,
    )
```

time: 88.4 us -> 83.7 us (0.947)
  Pallas kernels: 71 us -> 82.9 us
  local copies, waits for them, and re-layouts: 9.8 us -> 0 us
  other arithmetic: 6.58 us -> 0 us
    pallas_call x1 -> x2, Pallas kernels: 71 us -> 82.9 us  [the longest x1 79.3 us: per_device(): pl.pallas_call(layer_kernel, name='layer', out_shape=jax.ShapeDtypeStruct...]
    unnamed x9 -> x0, local copies, waits for them, and re-layouts: 7.21 us -> none
    another operation x3 -> x0, other arithmetic: 2.53 us -> none  [the longest x2 1.91 us: per_device(): jnp.stack([jnp.concatenate([dense_gate.T, gate_vector[None], jnp.zeros((3...]
    reduce_sum x2 -> x0, other arithmetic: 1.61 us -> none  [the longest x1 0.92 us: routing_block(): rank = jnp.sum((same & before).astype(F32), axis=(2, 3))]
    reshape x1 -> x0, local copies, waits for them, and re-layouts: 0.96 us -> none  [per_device(): dd = jnp.pad(dense_down.reshape(2, 44, HALF), ((0, 0), (0, 4), (0, 0)))]
where the time goes in v2:
time: 83.7 us; the launch traced here: 83.6 us
  Pallas kernels  82.9 us (99%)
    pallas_call x1, Pallas kernels, per_device(): pl.pallas_call(layer_kernel, name='layer', out_shape=jax.ShapeDtypeStruct...  79.3 us
    pallas_call x1, Pallas kernels, per_device(): pl.pallas_call(split_kernel, name='split', out_shape=(jax.ShapeDtypeStruc...  3.61 us

profile of v2, /device:TPU:0, one launch (start us, length us, event | category | flops | bytes accessed | tf_op | source)
XLA Modules:
  0.0 83.6 jit_solution(1685459295140244529)
XLA Ops:
  0.6 79.3 %layer.1.both = bf16[32,1280]{1,0:T(8,128)(2,1)} custom-call(bf16[32,2048]{1,0:T(8,128)(2,1)} %hid.1, f32[1,128]{1,0:T(1,128)} %constant.2.clone.freq, s32[32]{0:T(128)} %plen.1, s32[1,32]{1,0:T(1,128)} %bitcast.18, f32[1,2048]{1,0:T(1,128)} %bitcast.15, f32[8]{0:T(128)} %lam.1, f32[1,128]{1,0:T(1,128)} %bitcast.21, f32[1,2048]{1,0:T(1,128)} %bitcast.16, ...), custom_call_target="tpu_custom_call" | custom-call | tf_op jit(solution)/shard_map/layer/pallas_call | solution.py:575
  80.0 3.6 %split.1 = (bf16[32,1024]{1,0:T(8,128)(2,1)}, bf16[32,128]{1,0:T(8,128)(2,1)}, bf16[32,128]{1,0:T(8,128)(2,1)}) custom-call(bf16[32,1280]{1,0:T(8,128)(2,1)} %layer.1.both), custom_call_target="tpu_custom_call" | custom-call | tf_op jit(solution)/shard_map/split/pallas_call | solution.py:593

commit v3 on v2

v3 whole, which is shorter than its diff:
```python
import jax
import jax.numpy as jnp
import numpy as np
from jax import lax
from jax.experimental import pallas as pl
from jax.experimental.pallas import tpu as pltpu
from jax.sharding import PartitionSpec as P

EPS = 1e-05
ROPE_BASE = 10000.0
BF = jnp.bfloat16
F32 = jnp.float32
ROWS = 32
WIDTH = 2048
HALF = 1024
CACHE = 1024
GRP = 4
NGRP = ROWS // GRP
AHEAD = 3
VMEM_BYTES = 66 * 1000 * 1000
NEAR = (1, 3, 2)
NT = (((1,), (1,)), ((), ()))
TN = (((0,), (0,)), ((), ()))


def dot(a, b):
    return jnp.dot(a, b, preferred_element_type=F32)


def dot_nt(a, b):
    return lax.dot_general(a, b, NT, preferred_element_type=F32)


def dot_tn(a, b):
    return lax.dot_general(a, b, TN, preferred_element_type=F32)


def layer_kernel(
    hid, freq, plen, prow, again, lam, hgain, fgain, ids, wts, gvec,
    kc_h, vc_h, wq_h, wk_h, wv_h, wo_h, eg_h, eu_h, ed_h, dg_h, du_h, dd_h,
    out,
    kb, vb, wq, wk, wv, wo, eg, eu, ed, dg, du, dtail,
    wdg, ddg, qs, kn, vn, ho, pbuf, resid, rt, G, D, X, Xo, abuf, Y, R,
    dact, gsc, sel, selw, pb, s1, tb, s2,
    lsem, kvsem, wss, wrs, tps, tpr, rts, rtr,
    gss, grs, gds, gdr, zs, zr, xds, xdr, as_, ar, das, dar, ys, yr,
    r1s, r1r, r2s, r2r,
):
    c = lax.axis_index("tp")
    ep = lax.axis_index("ep")
    z = ep // 16
    p0 = ep % 16
    y = p0 // 4
    x = p0 % 4
    sa = 1 + 3 * c
    sb = 4 - 3 * c
    a = x * (1 - c) + y * c
    b = y * (1 - c) + x * c
    zb = z * 16
    other = 1 - c
    half = pl.ds(pl.multiple_of(c * HALF, HALF), HALF)
    other_half = pl.ds(pl.multiple_of(other * HALF, HALF), HALF)

    def local(src, dst, sem):
        return pltpu.make_async_copy(src, dst, sem)

    def remote(src, dst, ssem, rsem, **dev):
        return pltpu.make_async_remote_copy(
            src_ref=src, dst_ref=dst, send_sem=ssem, recv_sem=rsem,
            device_id=dev, device_id_type=pl.DeviceIdType.MESH,
        )

    def pidx(aa, bb):
        return aa * sa + bb * sb

    def z_ep(step):
        return ((z + 4 + step) % 4) * 16 + p0

    own_w = [
        local(dg_h, dg, lsem.at[3]),
        local(du_h, du, lsem.at[4]),
        local(dd_h.at[pl.ds(0, 48)], ddg.at[0, z], lsem.at[9]),
        local(dd_h.at[pl.ds(40, 48)], dtail, lsem.at[10]),
    ]
    first = [
        local(wk_h, wk, lsem.at[1]),
        local(wv_h, wv, lsem.at[2]),
        local(wq_h, wq, lsem.at[0]),
    ]
    for cp in own_w + first:
        cp.start()

    def kv(g):
        rows = pl.ds(g * GRP, GRP)
        return (
            local(kc_h.at[rows], kb.at[rows], kvsem.at[0, g]),
            local(vc_h.at[rows], vb.at[rows], kvsem.at[1, g]),
        )

    for g in range(AHEAD):
        for cp in kv(g):
            cp.start()

    later = [
        local(wo_h, wo, lsem.at[5]),
        local(eg_h.at[0], eg, lsem.at[6]),
        local(eu_h.at[0], eu, lsem.at[7]),
        local(ed_h.at[0], ed, lsem.at[8]),
    ]

    barrier = pltpu.get_barrier_semaphore()
    for k in range(1, 16):
        dest = zb + ((y + k // 4) % 4) * 4 + (x + k % 4) % 4
        pl.semaphore_signal(barrier, inc=1, device_id={"ep": dest}, device_id_type=pl.DeviceIdType.MESH)
    for step in NEAR:
        pl.semaphore_signal(barrier, inc=1, device_id={"ep": z_ep(step)}, device_id_type=pl.DeviceIdType.MESH)
    pl.semaphore_signal(barrier, inc=1, device_id={"tp": other}, device_id_type=pl.DeviceIdType.MESH)

    for cp in own_w:
        cp.wait()
    gv = gvec[...].astype(F32)
    gv = jnp.concatenate([gv[i : i + 1] for i in range(16)], axis=1)
    pad_row = lax.broadcasted_iota(jnp.int32, (4, WIDTH), 0)
    wdg[0, z, 0:44, :] = dg[...]
    wdg[0, z, 44:48, :] = jnp.where(pad_row == 0, gv, 0.0).astype(BF)
    wdg[1, z, 0:44, :] = du[...]
    wdg[1, z, 44:48, :] = jnp.zeros((4, WIDTH), BF)
    ddg[1, z] = pltpu.roll(dtail[...].astype(F32), 44, 0).astype(BF)

    at = lax.broadcasted_iota(jnp.int32, (ROWS, 128), 0)
    lane = lax.broadcasted_iota(jnp.int32, (ROWS, 128), 1)
    diag = at == lane
    shifted = at + 32 * a == lane

    def lanes(v, fill):
        return jnp.concatenate([v.astype(F32), jnp.full((v.shape[0], 128 - ROWS), fill, F32)], axis=1)

    def column(v):
        return jnp.sum(jnp.where(diag, v, 0.0), axis=1, keepdims=True)

    def moved(col):
        return jnp.sum(jnp.where(shifted, col, 0.0), axis=0, keepdims=True)

    id_rows = lanes(ids[...], -1.0)
    wt_rows = lanes(wts[...], 0.0)
    earlier = lane < at
    facts = []
    for k in range(2):
        col = column(id_rows[k : k + 1])
        same = jnp.where(id_rows[0:1] == col, 1.0, 0.0) + jnp.where(id_rows[1:2] == col, 1.0, 0.0)
        rank = jnp.sum(jnp.where(earlier, same, 0.0), axis=1, keepdims=True)
        facts.append(moved(col * 4.0 + rank))
    for k in range(2):
        facts.append(moved(column(wt_rows[k : k + 1])))
    facts.append(jnp.zeros((4, 128), F32))
    rt[p0] = jnp.concatenate(facts, axis=0)

    pl.semaphore_wait(barrier, 19)

    def rt_copy(k):
        dest = zb + ((y + k // 4) % 4) * 4 + (x + k % 4) % 4
        return remote(rt.at[p0], rt.at[p0], rts.at[k], rtr.at[k], ep=dest)

    for k in range(1, 16):
        rt_copy(k).start()

    def w_copy(i):
        block = (z + 4 + (0, 0, 0, 0, -1, 1, -1, 1)[i]) % 4
        ref = (
            wdg.at[:, block], wdg.at[:, block], ddg.at[:, block], ddg.at[:, block],
            wdg.at[0, block], wdg.at[1, block], ddg.at[0, block], ddg.at[1, block],
        )[i]
        return remote(ref, ref, wss.at[i], wrs.at[i], ep=z_ep((1, -1)[i % 2]))

    def w_wait(i):
        block = (z + 4 + (-1, 1, -1, 1, -2, 2, -2, 2)[i]) % 4
        ref = (
            wdg.at[:, block], wdg.at[:, block], ddg.at[:, block], ddg.at[:, block],
            wdg.at[0, block], wdg.at[1, block], ddg.at[0, block], ddg.at[1, block],
        )[i]
        remote(ref, ref, wss.at[i], wrs.at[i], tp=other).wait_recv()

    for i in (2, 3, 0, 1):
        w_copy(i).start()

    h = hid[...].astype(F32)
    normed = (h * lax.rsqrt(jnp.mean(h * h, axis=-1, keepdims=True) + EPS) * again[...]).astype(BF)
    angles = column(lanes(prow[...], 0.0)) * freq[...]
    cos = jnp.cos(angles)
    low = (lane & 63) < 32
    sin = jnp.sin(angles) * jnp.where(low, -1.0, 1.0)

    def rotated(v):
        turned = jnp.where(low, pltpu.roll(v, 96, 1), pltpu.roll(v, 32, 1))
        return (v * cos + turned * sin).astype(BF)

    for cp in first:
        cp.wait()
    new_k = rotated(dot(normed, wk[...]))
    new_v = dot(normed, wv[...]).astype(BF)
    out[:, HALF : HALF + 128] = new_k
    out[:, HALF + 128 : HALF + 256] = new_v
    kn[...] = new_k.astype(F32)
    vn[...] = new_v.astype(F32)
    q = dot(normed, wq[...])
    for i in range(8):
        qs[:, i, :] = rotated(q[:, i * 128 : (i + 1) * 128]).astype(F32) * 0.125

    lam_col = jnp.zeros((8, 128), F32)
    rows8 = lax.broadcasted_iota(jnp.int32, (8, 128), 0)
    for i in range(8):
        lam_col = jnp.where(rows8 == i, lam[i], lam_col)
    left = lax.broadcasted_iota(jnp.int32, (8, 128), 1) < 64
    last16 = lax.broadcasted_iota(jnp.int32, (16, 128), 0) == 15
    places = lax.broadcasted_iota(jnp.int32, (16, CACHE), 1)
    gain = hgain[...]

    @pl.loop(0, NGRP)
    def _(g):
        for cp in kv(g):
            cp.wait()

        @pl.when(g + AHEAD < NGRP)
        def _():
            for cp in kv(g + AHEAD):
                cp.start()

        @pl.when(g + AHEAD == NGRP)
        def _():
            later[0].start()

        for i in range(GRP):
            s = g * GRP + i
            tail = pl.ds(CACHE - 16, 16)
            kb[s, tail, :] = jnp.where(
                last16, jnp.broadcast_to(kn[pl.ds(s, 1), :], (16, 128)), kb[s, tail, :].astype(F32)
            ).astype(BF)
            vb[s, tail, :] = jnp.where(
                last16, jnp.broadcast_to(vn[pl.ds(s, 1), :], (16, 128)), vb[s, tail, :].astype(F32)
            ).astype(BF)
            qv = qs[s]
            q2 = jnp.concatenate(
                [jnp.where(left, qv, 0.0), jnp.where(left, 0.0, qv)], axis=0
            ).astype(BF)
            scores = dot_nt(q2, kb[s])
            usable = (places < plen[s]) | (places == CACHE - 1)
            scores = jnp.where(usable, scores, -jnp.inf)
            peak = jnp.max(scores, axis=-1, keepdims=True)
            weights = jnp.exp(scores - peak)
            total = jnp.sum(weights, axis=-1, keepdims=True)
            mapped = dot(weights.astype(BF), vb[s]) / total
            mix = mapped[0:8] - lam_col * mapped[8:16]
            ho[s] = mix * lax.rsqrt(jnp.mean(mix * mix, axis=-1, keepdims=True) + EPS) * gain

    for cp in later[1:]:
        cp.start()
    later[0].wait()
    head_out = jnp.concatenate([ho[:, i, :].astype(BF) for i in range(8)], axis=1)
    pbuf[0] = dot(head_out, wo[...]).astype(BF)
    tp_copy = remote(pbuf.at[0], pbuf.at[1], tps, tpr, tp=other)
    tp_copy.start()
    tp_copy.wait()
    attn_out = (pbuf[0].astype(F32) + pbuf[1].astype(F32)).astype(BF)
    res = hid[...].astype(F32) + attn_out.astype(F32)
    resid[...] = res
    G[b * 4 + a] = (
        res * lax.rsqrt(jnp.mean(res * res, axis=-1, keepdims=True) + EPS) * fgain[...]
    ).astype(BF)

    def g_copy(ka, kb_, da, db):
        src = ((b + 4 - kb_) % 4) * 4 + (a + 4 - ka) % 4
        dest = zb + pidx((a + da) % 4, (b + db) % 4)
        i = (ka + da) * 4 + kb_ + db
        ref = G.at[src, :, half]
        return remote(ref, ref, gss.at[i], grs.at[i], ep=dest)

    def g_share(ka, kb_):
        aa, bb = (a + 4 - ka) % 4, (b + 4 - kb_) % 4
        i = kb_ * 4 + ka
        return remote(
            G.at[bb * 4 + aa, :, half], G.at[aa * 4 + bb, :, half], gds.at[i], gdr.at[i], tp=other
        )

    def g_arrive(ka, kb_):
        i = ka * 4 + kb_
        ref = G.at[((b + 4 - kb_) % 4) * 4 + (a + 4 - ka) % 4, :, half]
        remote(ref, ref, gss.at[i], grs.at[i], tp=other).wait_recv()
        g_share(ka, kb_).start()

    for k in NEAR:
        g_copy(0, 0, k, 0).start()
        g_copy(0, 0, 0, k).start()

    for i in (2, 3):
        w_wait(i)
        w_copy(4 + i).start()

    for k in range(1, 16):
        src = ((y + 4 - k // 4) % 4) * 4 + (x + 4 - k % 4) % 4
        remote(rt.at[src], rt.at[src], rts.at[k], rtr.at[k], tp=other).wait_recv()
    row = lax.broadcasted_iota(jnp.int32, (64, 128), 0)
    token = lax.broadcasted_iota(jnp.int32, (64, 128), 1)
    target = ((((row >> 4) * 16 + p0) >> 1) * 4 + (row & 3)).astype(F32)
    mine = ((row >> 2) & 3) == (token >> 5)
    for i in range(4):
        facts = rt[pidx(0, i)] + rt[pidx(1, i)] + rt[pidx(2, i)] + rt[pidx(3, i)]
        hit0 = mine & (facts[0:1] == target)
        hit1 = mine & (facts[1:2] == target)
        sel[i] = jnp.where(hit0 | hit1, 1.0, 0.0).astype(BF)
        selw[i] = (jnp.where(hit0, facts[2:3], 0.0) + jnp.where(hit1, facts[3:4], 0.0)).astype(BF)

    def z_copy(k, kb_):
        to, g = (z + k) % 4, (b + 4 - kb_) % 4
        return remote(D.at[to, g], X.at[z, g], zs.at[k, kb_], zr.at[k, kb_], ep=to * 16 + p0)

    def select(kb_):
        g = (b + 4 - kb_) % 4
        rows_ = dot(sel[g], G[pl.ds(g * 4, 4), :, half].reshape(128, HALF))
        rows_ = rows_.astype(BF).reshape(4, 16, HALF)
        for i in range(4):
            D[i, g] = rows_[i]
        for k in NEAR:
            z_copy(k, kb_).start()

    for ka in NEAR:
        g_arrive(ka, 0)
    for k in NEAR:
        for ka in NEAR:
            g_copy(ka, 0, 0, k).start()
    select(0)
    for k in NEAR:
        for ka in (0, 1, 3, 2):
            g_arrive(ka, k)
        select(k)
        if k == 1:
            for i in (0, 1):
                w_wait(i)
                w_copy(4 + i).start()
    X[z] = D[z]

    def x_share(k):
        src = (z + 4 - k) % 4
        return remote(X.at[src], Xo.at[src], xds.at[k], xdr.at[k], tp=other)

    x_share(0).start()

    for i in range(4, 8):
        w_wait(i)
    for ka in range(4):
        for kb_ in range(4):
            if ka or kb_:
                i = ka * 4 + kb_
                ref = G.at[((b + 4 - kb_) % 4) * 4 + (a + 4 - ka) % 4, :, other_half]
                remote(ref, ref, gds.at[i], gdr.at[i], tp=other).wait_recv()

    @pl.loop(0, 4)
    def _(g):
        tokens = G[pl.ds(g * 4, 4)].reshape(128, WIDTH)
        pre_gate = dot_nt(tokens, wdg[0].reshape(192, WIDTH))
        pre_up = dot_nt(tokens, wdg[1].reshape(192, WIDTH))
        act = pre_gate / (1.0 + jnp.exp(-pre_gate)) * pre_up
        act = jnp.concatenate([act, jnp.zeros((128, 64), F32)], axis=1).astype(BF)
        dact[0, pl.ds(g * 4, 4)] = act.reshape(4, ROWS, 256)
        mix_gate = (1.0 / (1.0 + jnp.exp(-pre_gate[:, 44:45]))).astype(BF).astype(F32)
        gsc[g] = jnp.broadcast_to(mix_gate, (128, 128))

    act_copy = remote(dact.at[0], dact.at[1], das, dar, tp=other)
    act_copy.start()

    for k in NEAR:
        src = (z + 4 - k) % 4
        for kb_ in (0, 1, 3, 2):
            ref = X.at[src, (b + 4 - kb_) % 4]
            remote(ref, ref, zs.at[k, kb_], zr.at[k, kb_], tp=other).wait_recv()
        x_share(k).start()
    for cp in later[1:]:
        cp.wait()
    rr = lax.broadcasted_iota(jnp.int32, (256, 256), 0)
    cc = lax.broadcasted_iota(jnp.int32, (256, 256), 1)
    swap = (rr & 195) + ((rr >> 2) & 12) + ((rr & 12) << 2) == cc
    swap = jnp.where(swap, 1.0, 0.0).astype(BF)
    own_rows = X[...].reshape(256, HALF)
    gate_pre = dot_nt(own_rows, eg[:, half])
    up_pre = dot_nt(own_rows, eu[:, half])
    for k in (0, 1, 3, 2):
        ref = Xo.at[(z + 4 - k) % 4]
        remote(ref, ref, xds.at[k], xdr.at[k], tp=other).wait_recv()
    rows_in = dot(swap, Xo[...].reshape(256, HALF)).astype(BF)
    gate_pre = gate_pre + dot_nt(rows_in, eg[:, other_half])
    up_pre = up_pre + dot_nt(rows_in, eu[:, other_half])
    inner = gate_pre / (1.0 + jnp.exp(-gate_pre)) * up_pre
    abuf[0] = jnp.concatenate([inner, jnp.zeros((256, 32), F32)], axis=1).astype(BF)
    a_copy = remote(abuf.at[0], abuf.at[1], as_, ar, tp=other)
    a_copy.start()
    own_ed = ed[pl.ds(pl.multiple_of(c * 352, 32), 352), :]
    other_ed = ed[pl.ds(pl.multiple_of(other * 352, 32), 352), :]
    down = dot(abuf[0][:, :352], own_ed)
    remote(abuf.at[0], abuf.at[1], as_, ar, tp=other).wait_recv()
    other_act = dot(swap, abuf[1]).astype(BF)
    down = down + dot(other_act[:, :352], other_ed)
    Y[...] = down.astype(BF).reshape(4, 4, 16, HALF)

    def y_copy(k, kb_):
        to, g = (z + k) % 4, (b + kb_) % 4
        return remote(Y.at[to, g], R.at[z, g], ys.at[k, kb_], yr.at[k, kb_], ep=to * 16 + p0)

    for kb_ in (1, 3, 2, 0):
        for k in NEAR:
            y_copy(k, kb_).start()
    R[z] = Y[z]
    remote(dact.at[0], dact.at[1], das, dar, tp=other).wait_recv()

    def r1_copy(k):
        to = (b + k) % 4
        return remote(pb.at[to], s1.at[k - 1], r1s.at[k], r1r.at[k], ep=zb + pidx(a, to))

    def r2_copy(k):
        to = (a + k) % 4
        return remote(tb.at[to], s2.at[k - 1], r2s.at[k], r2r.at[k], ep=zb + pidx(to, b))

    for kb_ in (1, 3, 2, 0):
        g = (b + kb_) % 4
        other_act = jnp.concatenate([dact[1, i * 4 + g] for i in range(4)], axis=0)
        part = dot(dact[0, pl.ds(g * 4, 4)].reshape(128, 256)[:, :192], ddg[c].reshape(192, HALF)) + dot(
            other_act[:, :192], ddg[other].reshape(192, HALF)
        )
        for k in NEAR:
            ref = R.at[(z + 4 - k) % 4, g]
            remote(ref, ref, ys.at[k, kb_], yr.at[k, kb_], tp=other).wait_recv()
        rows_back = jnp.concatenate([R[i, g] for i in range(4)], axis=0)
        part = part * gsc[g][:, 0:1] + dot_tn(selw[g], rows_back)
        pb[g] = part.astype(BF).reshape(4, ROWS, HALF)
        if kb_:
            r1_copy(kb_).start()
    for k in NEAR:
        r1_copy(k).wait_recv()
    tb[...] = (
        pb[b].astype(F32) + s1[0].astype(F32) + s1[1].astype(F32) + s1[2].astype(F32)
    ).astype(BF)
    for k in NEAR:
        r2_copy(k).start()
    for k in NEAR:
        r2_copy(k).wait_recv()
    final = tb[a].astype(F32) + s2[0].astype(F32) + s2[1].astype(F32) + s2[2].astype(F32)
    out[:, :HALF] = (resid[:, half] + final).astype(BF)

    for k in range(1, 16):
        rt_copy(k).wait_send()
    for i in range(8):
        w_copy(i).wait_send()
    for k in NEAR:
        g_copy(0, 0, k, 0).wait_send()
        g_copy(0, 0, 0, k).wait_send()
        r1_copy(k).wait_send()
        r2_copy(k).wait_send()
        for i in range(4):
            z_copy(k, i).wait_send()
            y_copy(k, i).wait_send()
            if i:
                g_copy(i, 0, 0, k).wait_send()
    for i in range(1, 16):
        g_share(i // 4, i % 4).wait_send()
    for k in range(4):
        x_share(k).wait_send()
    act_copy.wait_send()
    a_copy.wait_send()


def split_kernel(both, out, nk, nv, sem):
    copies = [
        pltpu.make_async_copy(both.at[:, pl.ds(0, HALF)], out, sem.at[0]),
        pltpu.make_async_copy(both.at[:, pl.ds(HALF, 128)], nk, sem.at[1]),
        pltpu.make_async_copy(both.at[:, pl.ds(HALF + 128, 128)], nv, sem.at[2]),
    ]
    for cp in copies:
        cp.start()
    for cp in copies:
        cp.wait()


def per_device(
    hidden_in, past_lengths, key_cache, value_cache, attn_gain, w_query, w_key, w_value,
    lambdas, head_gain, w_out, ffn_gain, route_ids, route_weights, expert_gate, expert_up,
    expert_down, gate_vector, dense_gate, dense_up, dense_down,
):
    freq = np.power(np.float32(ROPE_BASE), -(np.arange(128) % 32).astype(np.float32) / np.float32(32))
    freq = jnp.asarray(freq.astype(np.float32)[None])
    vm = pl.BlockSpec(memory_space=pltpu.VMEM)
    sm = pl.BlockSpec(memory_space=pltpu.SMEM)
    hbm = pl.BlockSpec(memory_space=pl.ANY)
    V = pltpu.VMEM
    dma = pltpu.SemaphoreType.DMA
    scratch = [
        V((ROWS, CACHE, 128), BF), V((ROWS, CACHE, 128), BF),
        V((WIDTH, 1024), BF), V((WIDTH, 128), BF), V((WIDTH, 128), BF), V((1024, WIDTH), BF),
        V((352, WIDTH), BF), V((352, WIDTH), BF), V((704, HALF), BF),
        V((44, WIDTH), BF), V((44, WIDTH), BF), V((48, HALF), BF),
        V((2, 4, 48, WIDTH), BF), V((2, 4, 48, HALF), BF),
        V((ROWS, 8, 128), F32), V((ROWS, 128), F32), V((ROWS, 128), F32), V((ROWS, 8, 128), F32),
        V((2, ROWS, WIDTH), BF), V((ROWS, WIDTH), F32), V((16, 8, 128), F32),
        V((16, ROWS, WIDTH), BF), V((4, 4, 16, HALF), BF), V((4, 4, 16, HALF), BF),
        V((4, 4, 16, HALF), BF), V((2, 256, 384), BF), V((4, 4, 16, HALF), BF),
        V((4, 4, 16, HALF), BF), V((2, 16, ROWS, 256), BF), V((4, 128, 128), F32),
        V((4, 64, 128), BF), V((4, 64, 128), BF), V((4, 4, ROWS, HALF), BF),
        V((3, 4, ROWS, HALF), BF), V((4, ROWS, HALF), BF), V((3, ROWS, HALF), BF),
        dma((11,)), dma((2, NGRP)), dma((8,)), dma((8,)), dma, dma,
        dma((16,)), dma((16,)),
        dma((16,)), dma((16,)), dma((16,)), dma((16,)), dma((4, 4)), dma((4, 4)), dma((4,)),
        dma((4,)), dma, dma, dma, dma, dma((4, 4)), dma((4, 4)),
        dma((4,)), dma((4,)), dma((4,)), dma((4,)),
    ]
    both = pl.pallas_call(
        layer_kernel,
        name="layer",
        out_shape=jax.ShapeDtypeStruct((ROWS, HALF + 256), BF),
        in_specs=[vm, vm, sm, vm, vm, sm, vm, vm, vm, vm, vm] + [hbm] * 12,
        out_specs=vm,
        scratch_shapes=scratch,
        compiler_params=pltpu.CompilerParams(
            collective_id=0, has_side_effects=True, vmem_limit_bytes=VMEM_BYTES
        ),
    )(
        hidden_in, freq, past_lengths, past_lengths.reshape(1, ROWS), attn_gain.reshape(1, WIDTH),
        lambdas, head_gain.reshape(1, 128), ffn_gain.reshape(1, WIDTH), route_ids.T,
        route_weights.T, gate_vector.reshape(16, 128),
        key_cache, value_cache, w_query, w_key, w_value, w_out,
        expert_gate.swapaxes(1, 2), expert_up.swapaxes(1, 2), expert_down,
        dense_gate.T, dense_up.T, dense_down,
    )
    return pl.pallas_call(
        split_kernel,
        name="split",
        out_shape=(
            jax.ShapeDtypeStruct((ROWS, HALF), BF),
            jax.ShapeDtypeStruct((ROWS, 128), BF),
            jax.ShapeDtypeStruct((ROWS, 128), BF),
        ),
        in_specs=[hbm],
        out_specs=(hbm, hbm, hbm),
        scratch_shapes=[dma((3,))],
        compiler_params=pltpu.CompilerParams(vmem_limit_bytes=1 << 20),
    )(both)


def solution(mesh):
    return jax.shard_map(
        per_device,
        mesh=mesh,
        in_specs=(
            P("ep", None), P("ep"), P("ep", None, "tp"), P("ep", None, "tp"), P(),
            P(None, "tp"), P(None, "tp"), P(None, "tp"), P("tp"), P(), P("tp", None), P(),
            P("ep", None), P("ep", None), P("ep", None, "tp"), P("ep", None, "tp"),
            P("ep", None, "tp"), P(), P(None, ("ep", "tp")), P(None, ("ep", "tp")), P("ep", "tp"),
        ),
        out_specs=(P("ep", "tp"), P("ep", "tp"), P("ep", "tp")),
        check_vma=False,
    )
```

time: 83.7 us -> 76.6 us (0.915)
  the two profiles are of different devices: /device:TPU:0 before, /device:TPU:24 now
where the time goes in v3:
time: 76.6 us; the launch traced here: 76.4 us
  Pallas kernels  74.9 us (98%)
  local copies, waits for them, and re-layouts  0.88 us (1%)
    pallas_call x1, Pallas kernels, per_device(): pl.pallas_call(layer_kernel, name='layer', out_shape=jax.ShapeDtypeStruct...  74.2 us

profile of v3, /device:TPU:24, one launch (start us, length us, event | category | flops | bytes accessed | tf_op | source)
XLA Modules:
  0.0 76.4 jit_solution(15422439446414298248)
XLA Ops:
  0.6 74.2 %layer.1.both = bf16[32,1280]{1,0:T(8,128)(2,1)} custom-call(bf16[32,2048]{1,0:T(8,128)(2,1)} %hid.1, f32[1,128]{1,0:T(1,128)} %constant.2.clone.freq, s32[32]{0:T(128)} %plen.1, s32[1,32]{1,0:T(1,128)} %bitcast.18, f32[1,2048]{1,0:T(1,128)} %bitcast.15, f32[8]{0:T(128)} %lam.1, f32[1,128]{1,0:T(1,128)} %bitcast.21, f32[1,2048]{1,0:T(1,128)} %bitcast.16, ...), custom_call_target="tpu_custom_call" | custom-call | tf_op jit(solution)/shard_map/layer/pallas_call | solution.py:512
  74.9 0.0 copy-start
  74.9 0.9 %copy-done = bf16[32,1280]{1,0:T(8,128)(2,1)S(1)} copy-done((bf16[32,1280]{1,0:T(8,128)(2,1)S(1)}, bf16[32,1280]{1,0:T(8,128)(2,1)}, u32[]{:S(2)}) %copy-start) | copy-done | bytes 81944
  75.8 0.7 split.1
Async XLA Ops:
  74.9 0.9 %copy-start = (bf16[32,1280]{1,0:T(8,128)(2,1)S(1)}, bf16[32,1280]{1,0:T(8,128)(2,1)}, u32[]{:S(2)}) copy-start(bf16[32,1280]{1,0:T(8,128)(2,1)} %layer.1.both) | copy-start | bytes 245764

commit v4 on v3

--- a/solution.py
+++ b/solution.py
@@ -19,6 +19,7 @@
 AHEAD = 3
 VMEM_BYTES = 66 * 1000 * 1000
 NEAR = (1, 3, 2)
+MATES = tuple((i // 4, i % 4) for i in (10, 6, 14, 9, 11, 2, 8, 5, 7, 13, 15, 1, 3, 4, 12))
 NT = (((1,), (1,)), ((), ()))
 TN = (((0,), (0,)), ((), ()))
 
@@ -40,11 +41,11 @@
     kc_h, vc_h, wq_h, wk_h, wv_h, wo_h, eg_h, eu_h, ed_h, dg_h, du_h, dd_h,
     out,
     kb, vb, wq, wk, wv, wo, eg, eu, ed, dg, du, dtail,
-    wdg, ddg, qs, kn, vn, ho, pbuf, resid, rt, G, D, X, Xo, abuf, Y, R,
+    wdg, ddg, qs, kn, vn, ho, pbuf, resid, rt, G, zg, D, X, Xo, abuf, Y, R, M, m_in,
     dact, gsc, sel, selw, pb, s1, tb, s2,
     lsem, kvsem, wss, wrs, tps, tpr, rts, rtr,
-    gss, grs, gds, gdr, zs, zr, xds, xdr, as_, ar, das, dar, ys, yr,
-    r1s, r1r, r2s, r2r,
+    gss, grs, gds, gdr, zs, zr, xs, xr, xds, xdr, as_, ar, das, dar, ys, yr,
+    r1s, r1r, r2s, r2r, ms, mr,
 ):
     c = lax.axis_index("tp")
     ep = lax.axis_index("ep")
@@ -130,7 +131,7 @@
     at = lax.broadcasted_iota(jnp.int32, (ROWS, 128), 0)
     lane = lax.broadcasted_iota(jnp.int32, (ROWS, 128), 1)
     diag = at == lane
-    shifted = at + 32 * a == lane
+    shifted = at + 32 * z == lane
 
     def lanes(v, fill):
         return jnp.concatenate([v.astype(F32), jnp.full((v.shape[0], 128 - ROWS), fill, F32)], axis=1)
@@ -153,15 +154,14 @@
     for k in range(2):
         facts.append(moved(column(wt_rows[k : k + 1])))
     facts.append(jnp.zeros((4, 128), F32))
-    rt[p0] = jnp.concatenate(facts, axis=0)
+    rt[z] = jnp.concatenate(facts, axis=0)
 
     pl.semaphore_wait(barrier, 19)
 
     def rt_copy(k):
-        dest = zb + ((y + k // 4) % 4) * 4 + (x + k % 4) % 4
-        return remote(rt.at[p0], rt.at[p0], rts.at[k], rtr.at[k], ep=dest)
-
-    for k in range(1, 16):
+        return remote(rt.at[z], rt.at[z], rts.at[k], rtr.at[k], ep=z_ep(k))
+
+    for k in NEAR:
         rt_copy(k).start()
 
     def w_copy(i):
@@ -229,6 +229,7 @@
         def _():
             later[0].start()
 
+        sums, parts = [], []
         for i in range(GRP):
             s = g * GRP + i
             tail = pl.ds(CACHE - 16, 16)
@@ -247,10 +248,16 @@
             scores = jnp.where(usable, scores, -jnp.inf)
             peak = jnp.max(scores, axis=-1, keepdims=True)
             weights = jnp.exp(scores - peak)
-            total = jnp.sum(weights, axis=-1, keepdims=True)
-            mapped = dot(weights.astype(BF), vb[s]) / total
-            mix = mapped[0:8] - lam_col * mapped[8:16]
-            ho[s] = mix * lax.rsqrt(jnp.mean(mix * mix, axis=-1, keepdims=True) + EPS) * gain
+            sums.append(jnp.sum(weights, axis=-1, keepdims=True))
+            parts.append(weights.astype(BF))
+        for i in range(0, GRP, 2):
+            s = g * GRP + i
+            values = jnp.concatenate([vb[s], vb[s + 1]], axis=1)
+            pair = dot(jnp.concatenate(parts[i : i + 2], axis=0), values)
+            for j in range(2):
+                mapped = pair[16 * j : 16 * j + 16, 128 * j : 128 * j + 128] / sums[i + j]
+                mix = mapped[0:8] - lam_col * mapped[8:16]
+                ho[s + j] = mix * lax.rsqrt(jnp.mean(mix * mix, axis=-1, keepdims=True) + EPS) * gain
 
     for cp in later[1:]:
         cp.start()
@@ -259,6 +266,9 @@
     pbuf[0] = dot(head_out, wo[...]).astype(BF)
     tp_copy = remote(pbuf.at[0], pbuf.at[1], tps, tpr, tp=other)
     tp_copy.start()
+    for i in (2, 3, 0, 1):
+        w_wait(i)
+        w_copy(4 + i).start()
     tp_copy.wait()
     attn_out = (pbuf[0].astype(F32) + pbuf[1].astype(F32)).astype(BF)
     res = hid[...].astype(F32) + attn_out.astype(F32)
@@ -287,63 +297,60 @@
         remote(ref, ref, gss.at[i], grs.at[i], tp=other).wait_recv()
         g_share(ka, kb_).start()
 
-    for k in NEAR:
+    own_block = G.at[b * 4 + a, :, half]
+
+    def zg_copy(k):
+        return remote(own_block, zg.at[z], zs.at[k], zr.at[k], ep=z_ep(k))
+
+    for k in NEAR:
+        zg_copy(k).start()
         g_copy(0, 0, k, 0).start()
         g_copy(0, 0, 0, k).start()
-
-    for i in (2, 3):
-        w_wait(i)
-        w_copy(4 + i).start()
-
-    for k in range(1, 16):
-        src = ((y + 4 - k // 4) % 4) * 4 + (x + 4 - k % 4) % 4
-        remote(rt.at[src], rt.at[src], rts.at[k], rtr.at[k], tp=other).wait_recv()
-    row = lax.broadcasted_iota(jnp.int32, (64, 128), 0)
-    token = lax.broadcasted_iota(jnp.int32, (64, 128), 1)
-    target = ((((row >> 4) * 16 + p0) >> 1) * 4 + (row & 3)).astype(F32)
+    zg[z] = G[b * 4 + a, :, half]
+
+    for k in NEAR:
+        ref = rt.at[(z + 4 - k) % 4]
+        remote(ref, ref, rts.at[k], rtr.at[k], tp=other).wait_recv()
+    facts = rt[0] + rt[1] + rt[2] + rt[3]
+    row = lax.broadcasted_iota(jnp.int32, (256, 128), 0)
+    token = lax.broadcasted_iota(jnp.int32, (256, 128), 1)
+    target = (((zb + (row >> 4)) >> 1) * 4 + (row & 3)).astype(F32)
     mine = ((row >> 2) & 3) == (token >> 5)
-    for i in range(4):
-        facts = rt[pidx(0, i)] + rt[pidx(1, i)] + rt[pidx(2, i)] + rt[pidx(3, i)]
-        hit0 = mine & (facts[0:1] == target)
-        hit1 = mine & (facts[1:2] == target)
-        sel[i] = jnp.where(hit0 | hit1, 1.0, 0.0).astype(BF)
-        selw[i] = (jnp.where(hit0, facts[2:3], 0.0) + jnp.where(hit1, facts[3:4], 0.0)).astype(BF)
-
-    def z_copy(k, kb_):
-        to, g = (z + k) % 4, (b + 4 - kb_) % 4
-        return remote(D.at[to, g], X.at[z, g], zs.at[k, kb_], zr.at[k, kb_], ep=to * 16 + p0)
-
-    def select(kb_):
-        g = (b + 4 - kb_) % 4
-        rows_ = dot(sel[g], G[pl.ds(g * 4, 4), :, half].reshape(128, HALF))
-        rows_ = rows_.astype(BF).reshape(4, 16, HALF)
-        for i in range(4):
-            D[i, g] = rows_[i]
-        for k in NEAR:
-            z_copy(k, kb_).start()
+    hit0 = mine & (facts[0:1] == target)
+    hit1 = mine & (facts[1:2] == target)
+    sel[...] = jnp.where(hit0 | hit1, 1.0, 0.0).astype(BF)
+    selw[...] = (jnp.where(hit0, facts[2:3], 0.0) + jnp.where(hit1, facts[3:4], 0.0)).astype(BF)
 
     for ka in NEAR:
         g_arrive(ka, 0)
     for k in NEAR:
         for ka in NEAR:
             g_copy(ka, 0, 0, k).start()
-    select(0)
+
+    def mate(dy, dx):
+        return ((y + 4 + dy) % 4) * 4 + (x + 4 + dx) % 4
+
+    def x_copy(dy, dx):
+        i = dy * 4 + dx
+        to = mate(dy, dx)
+        return remote(D.at[to], X.at[p0], xs.at[i], xr.at[i], ep=zb + to)
+
+    def y_copy(dy, dx):
+        i = dy * 4 + dx
+        to = mate(dy, dx)
+        return remote(Y.at[to], R.at[p0], ys.at[i], yr.at[i], ep=zb + to)
+
+    for k in NEAR:
+        ref = zg.at[(z + 4 - k) % 4]
+        remote(ref, ref, zs.at[k], zr.at[k], tp=other).wait_recv()
+    D[...] = dot(sel[...], zg[...].reshape(128, HALF)).astype(BF).reshape(16, 16, HALF)
+    for dy, dx in MATES:
+        x_copy(dy, dx).start()
+    X[p0] = D[p0]
+
     for k in NEAR:
         for ka in (0, 1, 3, 2):
             g_arrive(ka, k)
-        select(k)
-        if k == 1:
-            for i in (0, 1):
-                w_wait(i)
-                w_copy(4 + i).start()
-    X[z] = D[z]
-
-    def x_share(k):
-        src = (z + 4 - k) % 4
-        return remote(X.at[src], Xo.at[src], xds.at[k], xdr.at[k], tp=other)
-
-    x_share(0).start()
-
     for i in range(4, 8):
         w_wait(i)
     for ka in range(4):
@@ -367,27 +374,46 @@
     act_copy = remote(dact.at[0], dact.at[1], das, dar, tp=other)
     act_copy.start()
 
-    for k in NEAR:
-        src = (z + 4 - k) % 4
-        for kb_ in (0, 1, 3, 2):
-            ref = X.at[src, (b + 4 - kb_) % 4]
-            remote(ref, ref, zs.at[k, kb_], zr.at[k, kb_], tp=other).wait_recv()
-        x_share(k).start()
+    def x_share(dy):
+        rows = pl.ds(((y + 4 - dy) % 4) * 4, 4)
+        return remote(X.at[rows], Xo.at[rows], xds.at[dy], xdr.at[dy], tp=other)
+
+    for dy in (0, 1, 3, 2):
+        for dx in range(4):
+            if dy or dx:
+                i = dy * 4 + dx
+                ref = X.at[mate(-dy, -dx)]
+                remote(ref, ref, xs.at[i], xr.at[i], tp=other).wait_recv()
+        x_share(dy).start()
+
+    def r1_copy(k):
+        to = (b + k) % 4
+        return remote(pb.at[to], s1.at[k - 1], r1s.at[k], r1r.at[k], ep=zb + pidx(a, to))
+
+    def r2_copy(k):
+        to = (a + k) % 4
+        return remote(tb.at[to], s2.at[k - 1], r2s.at[k], r2r.at[k], ep=zb + pidx(to, b))
+
+    remote(dact.at[0], dact.at[1], das, dar, tp=other).wait_recv()
+    for kb_ in (1, 3, 2, 0):
+        g = (b + kb_) % 4
+        other_act = jnp.concatenate([dact[1, i * 4 + g] for i in range(4)], axis=0)
+        part = dot(dact[0, pl.ds(g * 4, 4)].reshape(128, 256)[:, :192], ddg[c].reshape(192, HALF)) + dot(
+            other_act[:, :192], ddg[other].reshape(192, HALF)
+        )
+        pb[g] = (part * gsc[g][:, 0:1]).astype(BF).reshape(4, ROWS, HALF)
+        if kb_:
+            r1_copy(kb_).start()
+
     for cp in later[1:]:
         cp.wait()
-    rr = lax.broadcasted_iota(jnp.int32, (256, 256), 0)
-    cc = lax.broadcasted_iota(jnp.int32, (256, 256), 1)
-    swap = (rr & 195) + ((rr >> 2) & 12) + ((rr & 12) << 2) == cc
-    swap = jnp.where(swap, 1.0, 0.0).astype(BF)
+    for dy in (0, 1, 3, 2):
+        rows = pl.ds(((y + 4 - dy) % 4) * 4, 4)
+        remote(X.at[rows], Xo.at[rows], xds.at[dy], xdr.at[dy], tp=other).wait_recv()
     own_rows = X[...].reshape(256, HALF)
-    gate_pre = dot_nt(own_rows, eg[:, half])
-    up_pre = dot_nt(own_rows, eu[:, half])
-    for k in (0, 1, 3, 2):
-        ref = Xo.at[(z + 4 - k) % 4]
-        remote(ref, ref, xds.at[k], xdr.at[k], tp=other).wait_recv()
-    rows_in = dot(swap, Xo[...].reshape(256, HALF)).astype(BF)
-    gate_pre = gate_pre + dot_nt(rows_in, eg[:, other_half])
-    up_pre = up_pre + dot_nt(rows_in, eu[:, other_half])
+    other_rows = Xo[...].reshape(256, HALF)
+    gate_pre = dot_nt(own_rows, eg[:, half]) + dot_nt(other_rows, eg[:, other_half])
+    up_pre = dot_nt(own_rows, eu[:, half]) + dot_nt(other_rows, eu[:, other_half])
     inner = gate_pre / (1.0 + jnp.exp(-gate_pre)) * up_pre
     abuf[0] = jnp.concatenate([inner, jnp.zeros((256, 32), F32)], axis=1).astype(BF)
     a_copy = remote(abuf.at[0], abuf.at[1], as_, ar, tp=other)
@@ -396,42 +422,12 @@
     other_ed = ed[pl.ds(pl.multiple_of(other * 352, 32), 352), :]
     down = dot(abuf[0][:, :352], own_ed)
     remote(abuf.at[0], abuf.at[1], as_, ar, tp=other).wait_recv()
-    other_act = dot(swap, abuf[1]).astype(BF)
-    down = down + dot(other_act[:, :352], other_ed)
-    Y[...] = down.astype(BF).reshape(4, 4, 16, HALF)
-
-    def y_copy(k, kb_):
-        to, g = (z + k) % 4, (b + kb_) % 4
-        return remote(Y.at[to, g], R.at[z, g], ys.at[k, kb_], yr.at[k, kb_], ep=to * 16 + p0)
-
-    for kb_ in (1, 3, 2, 0):
-        for k in NEAR:
-            y_copy(k, kb_).start()
-    R[z] = Y[z]
-    remote(dact.at[0], dact.at[1], das, dar, tp=other).wait_recv()
-
-    def r1_copy(k):
-        to = (b + k) % 4
-        return remote(pb.at[to], s1.at[k - 1], r1s.at[k], r1r.at[k], ep=zb + pidx(a, to))
-
-    def r2_copy(k):
-        to = (a + k) % 4
-        return remote(tb.at[to], s2.at[k - 1], r2s.at[k], r2r.at[k], ep=zb + pidx(to, b))
-
-    for kb_ in (1, 3, 2, 0):
-        g = (b + kb_) % 4
-        other_act = jnp.concatenate([dact[1, i * 4 + g] for i in range(4)], axis=0)
-        part = dot(dact[0, pl.ds(g * 4, 4)].reshape(128, 256)[:, :192], ddg[c].reshape(192, HALF)) + dot(
-            other_act[:, :192], ddg[other].reshape(192, HALF)
-        )
-        for k in NEAR:
-            ref = R.at[(z + 4 - k) % 4, g]
-            remote(ref, ref, ys.at[k, kb_], yr.at[k, kb_], tp=other).wait_recv()
-        rows_back = jnp.concatenate([R[i, g] for i in range(4)], axis=0)
-        part = part * gsc[g][:, 0:1] + dot_tn(selw[g], rows_back)
-        pb[g] = part.astype(BF).reshape(4, ROWS, HALF)
-        if kb_:
-            r1_copy(kb_).start()
+    down = down + dot(abuf[1][:, :352], other_ed)
+    Y[...] = down.astype(BF).reshape(16, 16, HALF)
+
+    for dy, dx in MATES:
+        y_copy(dy, dx).start()
+    R[p0] = Y[p0]
     for k in NEAR:
         r1_copy(k).wait_recv()
     tb[...] = (
@@ -439,27 +435,42 @@
     ).astype(BF)
     for k in NEAR:
         r2_copy(k).start()
+    for dy, dx in MATES:
+        i = dy * 4 + dx
+        ref = R.at[mate(-dy, -dx)]
+        remote(ref, ref, ys.at[i], yr.at[i], tp=other).wait_recv()
+    M[...] = dot_tn(selw[...], R[...].reshape(256, HALF)).astype(BF).reshape(4, ROWS, HALF)
+
+    def m_copy(k):
+        return remote(M.at[(z + k) % 4], m_in.at[k - 1], ms.at[k], mr.at[k], ep=z_ep(k))
+
+    for k in NEAR:
+        m_copy(k).start()
     for k in NEAR:
         r2_copy(k).wait_recv()
     final = tb[a].astype(F32) + s2[0].astype(F32) + s2[1].astype(F32) + s2[2].astype(F32)
-    out[:, :HALF] = (resid[:, half] + final).astype(BF)
-
-    for k in range(1, 16):
-        rt_copy(k).wait_send()
+    final = resid[:, half] + final + M[z].astype(F32)
+    for k in NEAR:
+        m_copy(k).wait_recv()
+    final = final + m_in[0].astype(F32) + m_in[1].astype(F32) + m_in[2].astype(F32)
+    out[:, :HALF] = final.astype(BF)
+
     for i in range(8):
         w_copy(i).wait_send()
     for k in NEAR:
+        rt_copy(k).wait_send()
+        zg_copy(k).wait_send()
+        m_copy(k).wait_send()
         g_copy(0, 0, k, 0).wait_send()
         g_copy(0, 0, 0, k).wait_send()
         r1_copy(k).wait_send()
         r2_copy(k).wait_send()
-        for i in range(4):
-            z_copy(k, i).wait_send()
-            y_copy(k, i).wait_send()
-            if i:
-                g_copy(i, 0, 0, k).wait_send()
-    for i in range(1, 16):
-        g_share(i // 4, i % 4).wait_send()
+        for i in NEAR:
+            g_copy(i, 0, 0, k).wait_send()
+    for dy, dx in MATES:
+        x_copy(dy, dx).wait_send()
+        y_copy(dy, dx).wait_send()
+        g_share(dy, dx).wait_send()
     for k in range(4):
         x_share(k).wait_send()
     act_copy.wait_send()
@@ -497,17 +508,18 @@
         V((44, WIDTH), BF), V((44, WIDTH), BF), V((48, HALF), BF),
         V((2, 4, 48, WIDTH), BF), V((2, 4, 48, HALF), BF),
         V((ROWS, 8, 128), F32), V((ROWS, 128), F32), V((ROWS, 128), F32), V((ROWS, 8, 128), F32),
-        V((2, ROWS, WIDTH), BF), V((ROWS, WIDTH), F32), V((16, 8, 128), F32),
-        V((16, ROWS, WIDTH), BF), V((4, 4, 16, HALF), BF), V((4, 4, 16, HALF), BF),
-        V((4, 4, 16, HALF), BF), V((2, 256, 384), BF), V((4, 4, 16, HALF), BF),
-        V((4, 4, 16, HALF), BF), V((2, 16, ROWS, 256), BF), V((4, 128, 128), F32),
-        V((4, 64, 128), BF), V((4, 64, 128), BF), V((4, 4, ROWS, HALF), BF),
-        V((3, 4, ROWS, HALF), BF), V((4, ROWS, HALF), BF), V((3, ROWS, HALF), BF),
+        V((2, ROWS, WIDTH), BF), V((ROWS, WIDTH), F32), V((4, 8, 128), F32),
+        V((16, ROWS, WIDTH), BF), V((4, ROWS, HALF), BF), V((16, 16, HALF), BF),
+        V((16, 16, HALF), BF), V((16, 16, HALF), BF), V((2, 256, 384), BF), V((16, 16, HALF), BF),
+        V((16, 16, HALF), BF), V((4, ROWS, HALF), BF), V((3, ROWS, HALF), BF),
+        V((2, 16, ROWS, 256), BF), V((4, 128, 128), F32), V((256, 128), BF), V((256, 128), BF),
+        V((4, 4, ROWS, HALF), BF), V((3, 4, ROWS, HALF), BF), V((4, ROWS, HALF), BF),
+        V((3, ROWS, HALF), BF),
         dma((11,)), dma((2, NGRP)), dma((8,)), dma((8,)), dma, dma,
-        dma((16,)), dma((16,)),
-        dma((16,)), dma((16,)), dma((16,)), dma((16,)), dma((4, 4)), dma((4, 4)), dma((4,)),
-        dma((4,)), dma, dma, dma, dma, dma((4, 4)), dma((4, 4)),
-        dma((4,)), dma((4,)), dma((4,)), dma((4,)),
+        dma((4,)), dma((4,)),
+        dma((16,)), dma((16,)), dma((16,)), dma((16,)), dma((4,)), dma((4,)), dma((16,)), dma((16,)),
+        dma((4,)), dma((4,)), dma, dma, dma, dma, dma((16,)), dma((16,)),
+        dma((4,)), dma((4,)), dma((4,)), dma((4,)), dma((4,)), dma((4,)),
     ]
     both = pl.pallas_call(
         layer_kernel,

time: 76.6 us -> 74.1 us (0.967)
  the two profiles are of different devices: /device:TPU:24 before, /device:TPU:0 now
where the time goes in v4:
time: 74.1 us; the launch traced here: 73.9 us
  Pallas kernels  72.4 us (98%)
  local copies, waits for them, and re-layouts  0.88 us (1%)
    pallas_call x1, Pallas kernels, per_device(): pl.pallas_call(layer_kernel, name='layer', out_shape=jax.ShapeDtypeStruct...  71.7 us

profile of v4, /device:TPU:0, one launch (start us, length us, event | category | flops | bytes accessed | tf_op | source)
XLA Modules:
  0.0 73.9 jit_solution(2564928052273732678)
XLA Ops:
  0.6 71.7 %layer.1.both = bf16[32,1280]{1,0:T(8,128)(2,1)} custom-call(bf16[32,2048]{1,0:T(8,128)(2,1)} %hid.1, f32[1,128]{1,0:T(1,128)} %constant.2.clone.freq, s32[32]{0:T(128)} %plen.1, s32[1,32]{1,0:T(1,128)} %bitcast.18, f32[1,2048]{1,0:T(1,128)} %bitcast.15, f32[8]{0:T(128)} %lam.1, f32[1,128]{1,0:T(1,128)} %bitcast.21, f32[1,2048]{1,0:T(1,128)} %bitcast.16, ...), custom_call_target="tpu_custom_call" | custom-call | tf_op jit(solution)/shard_map/layer/pallas_call | solution.py:524
  72.4 0.0 copy-start
  72.4 0.9 %copy-done = bf16[32,1280]{1,0:T(8,128)(2,1)S(1)} copy-done((bf16[32,1280]{1,0:T(8,128)(2,1)S(1)}, bf16[32,1280]{1,0:T(8,128)(2,1)}, u32[]{:S(2)}) %copy-start) | copy-done | bytes 81944
  73.3 0.7 split.1
Async XLA Ops:
  72.4 0.9 %copy-start = (bf16[32,1280]{1,0:T(8,128)(2,1)S(1)}, bf16[32,1280]{1,0:T(8,128)(2,1)}, u32[]{:S(2)}) copy-start(bf16[32,1280]{1,0:T(8,128)(2,1)} %layer.1.both) | copy-start | bytes 245764

commit v5 on v4

--- a/solution.py
+++ b/solution.py
@@ -14,9 +14,9 @@
 WIDTH = 2048
 HALF = 1024
 CACHE = 1024
-GRP = 4
+GRP = 8
 NGRP = ROWS // GRP
-AHEAD = 3
+AHEAD = 2
 VMEM_BYTES = 66 * 1000 * 1000
 NEAR = (1, 3, 2)
 MATES = tuple((i // 4, i % 4) for i in (10, 6, 14, 9, 11, 2, 8, 5, 7, 13, 15, 1, 3, 4, 12))
@@ -98,10 +98,6 @@
             local(vc_h.at[rows], vb.at[rows], kvsem.at[1, g]),
         )
 
-    for g in range(AHEAD):
-        for cp in kv(g):
-            cp.start()
-
     later = [
         local(wo_h, wo, lsem.at[5]),
         local(eg_h.at[0], eg, lsem.at[6]),
@@ -155,6 +151,10 @@
         facts.append(moved(column(wt_rows[k : k + 1])))
     facts.append(jnp.zeros((4, 128), F32))
     rt[z] = jnp.concatenate(facts, axis=0)
+
+    for g in range(AHEAD):
+        for cp in kv(g):
+            cp.start()
 
     pl.semaphore_wait(barrier, 19)
 
@@ -266,9 +266,6 @@
     pbuf[0] = dot(head_out, wo[...]).astype(BF)
     tp_copy = remote(pbuf.at[0], pbuf.at[1], tps, tpr, tp=other)
     tp_copy.start()
-    for i in (2, 3, 0, 1):
-        w_wait(i)
-        w_copy(4 + i).start()
     tp_copy.wait()
     attn_out = (pbuf[0].astype(F32) + pbuf[1].astype(F32)).astype(BF)
     res = hid[...].astype(F32) + attn_out.astype(F32)
@@ -303,9 +300,8 @@
         return remote(own_block, zg.at[z], zs.at[k], zr.at[k], ep=z_ep(k))
 
     for k in NEAR:
+        g_copy(0, 0, k, 0).start()
         zg_copy(k).start()
-        g_copy(0, 0, k, 0).start()
-        g_copy(0, 0, 0, k).start()
     zg[z] = G[b * 4 + a, :, half]
 
     for k in NEAR:
@@ -321,8 +317,15 @@
     sel[...] = jnp.where(hit0 | hit1, 1.0, 0.0).astype(BF)
     selw[...] = (jnp.where(hit0, facts[2:3], 0.0) + jnp.where(hit1, facts[3:4], 0.0)).astype(BF)
 
+    for i in (2, 3):
+        w_wait(i)
+        w_copy(4 + i).start()
+
     for ka in NEAR:
         g_arrive(ka, 0)
+        if ka == 1:
+            for k in NEAR:
+                g_copy(0, 0, 0, k).start()
     for k in NEAR:
         for ka in NEAR:
             g_copy(ka, 0, 0, k).start()
@@ -346,6 +349,9 @@
     D[...] = dot(sel[...], zg[...].reshape(128, HALF)).astype(BF).reshape(16, 16, HALF)
     for dy, dx in MATES:
         x_copy(dy, dx).start()
+    for i in (0, 1):
+        w_wait(i)
+        w_copy(4 + i).start()
     X[p0] = D[p0]
 
     for k in NEAR:

time: 74.1 us -> 66.4 us (0.90)
  Pallas kernels: 72.4 us -> 64.7 us
    pallas_call x1, Pallas kernels: 71.7 us -> 64.1 us  [per_device(): pl.pallas_call(layer_kernel, name='layer', out_shape=jax.ShapeDtypeStruct...]
where the time goes in v5:
time: 66.4 us; the launch traced here: 66.3 us
  Pallas kernels  64.7 us (97%)
  local copies, waits for them, and re-layouts  0.88 us (1%)
    pallas_call x1, Pallas kernels, per_device(): pl.pallas_call(layer_kernel, name='layer', out_shape=jax.ShapeDtypeStruct...  64.1 us

profile of v5, /device:TPU:0, one launch (start us, length us, event | category | flops | bytes accessed | tf_op | source)
XLA Modules:
  0.0 66.3 jit_solution(11849449766636625772)
XLA Ops:
  0.6 64.1 %layer.1.both = bf16[32,1280]{1,0:T(8,128)(2,1)} custom-call(bf16[32,2048]{1,0:T(8,128)(2,1)} %hid.1, f32[1,128]{1,0:T(1,128)} %constant.2.clone.freq, s32[32]{0:T(128)} %plen.1, s32[1,32]{1,0:T(1,128)} %bitcast.18, f32[1,2048]{1,0:T(1,128)} %bitcast.15, f32[8]{0:T(128)} %lam.1, f32[1,128]{1,0:T(1,128)} %bitcast.21, f32[1,2048]{1,0:T(1,128)} %bitcast.16, ...), custom_call_target="tpu_custom_call" | custom-call | tf_op jit(solution)/shard_map/layer/pallas_call | solution.py:530
  64.7 0.0 copy-start
  64.7 0.9 %copy-done = bf16[32,1280]{1,0:T(8,128)(2,1)S(1)} copy-done((bf16[32,1280]{1,0:T(8,128)(2,1)S(1)}, bf16[32,1280]{1,0:T(8,128)(2,1)}, u32[]{:S(2)}) %copy-start) | copy-done | bytes 81944
  65.6 0.7 split.1
Async XLA Ops:
  64.7 0.9 %copy-start = (bf16[32,1280]{1,0:T(8,128)(2,1)S(1)}, bf16[32,1280]{1,0:T(8,128)(2,1)}, u32[]{:S(2)}) copy-start(bf16[32,1280]{1,0:T(8,128)(2,1)} %layer.1.both) | copy-start | bytes 245764

commit v6 on v5

--- a/solution.py
+++ b/solution.py
@@ -16,9 +16,10 @@
 CACHE = 1024
 GRP = 8
 NGRP = ROWS // GRP
-AHEAD = 2
+AHEAD = 4
 VMEM_BYTES = 66 * 1000 * 1000
-NEAR = (1, 3, 2)
+NEAR = (2, 1, 3)
+FAR = (2, 1, 3)
 MATES = tuple((i // 4, i % 4) for i in (10, 6, 14, 9, 11, 2, 8, 5, 7, 13, 15, 1, 3, 4, 12))
 NT = (((1,), (1,)), ((), ()))
 TN = (((0,), (0,)), ((), ()))
@@ -43,7 +44,7 @@
     kb, vb, wq, wk, wv, wo, eg, eu, ed, dg, du, dtail,
     wdg, ddg, qs, kn, vn, ho, pbuf, resid, rt, G, zg, D, X, Xo, abuf, Y, R, M, m_in,
     dact, gsc, sel, selw, pb, s1, tb, s2,
-    lsem, kvsem, wss, wrs, tps, tpr, rts, rtr,
+    lsem, wqsem, kvsem, wss, wrs, tps, tpr, rts, rtr,
     gss, grs, gds, gdr, zs, zr, xs, xr, xds, xdr, as_, ar, das, dar, ys, yr,
     r1s, r1r, r2s, r2r, ms, mr,
 ):
@@ -86,7 +87,10 @@
     first = [
         local(wk_h, wk, lsem.at[1]),
         local(wv_h, wv, lsem.at[2]),
-        local(wq_h, wq, lsem.at[0]),
+    ]
+    first += [
+        local(wq_h.at[:, pl.ds(i * 256, 256)], wq.at[:, pl.ds(i * 256, 256)], wqsem.at[i])
+        for i in range(4)
     ]
     for cp in own_w + first:
         cp.start()
@@ -112,17 +116,6 @@
     for step in NEAR:
         pl.semaphore_signal(barrier, inc=1, device_id={"ep": z_ep(step)}, device_id_type=pl.DeviceIdType.MESH)
     pl.semaphore_signal(barrier, inc=1, device_id={"tp": other}, device_id_type=pl.DeviceIdType.MESH)
-
-    for cp in own_w:
-        cp.wait()
-    gv = gvec[...].astype(F32)
-    gv = jnp.concatenate([gv[i : i + 1] for i in range(16)], axis=1)
-    pad_row = lax.broadcasted_iota(jnp.int32, (4, WIDTH), 0)
-    wdg[0, z, 0:44, :] = dg[...]
-    wdg[0, z, 44:48, :] = jnp.where(pad_row == 0, gv, 0.0).astype(BF)
-    wdg[1, z, 0:44, :] = du[...]
-    wdg[1, z, 44:48, :] = jnp.zeros((4, WIDTH), BF)
-    ddg[1, z] = pltpu.roll(dtail[...].astype(F32), 44, 0).astype(BF)
 
     at = lax.broadcasted_iota(jnp.int32, (ROWS, 128), 0)
     lane = lax.broadcasted_iota(jnp.int32, (ROWS, 128), 1)
@@ -152,9 +145,27 @@
     facts.append(jnp.zeros((4, 128), F32))
     rt[z] = jnp.concatenate(facts, axis=0)
 
+    h = hid[...].astype(F32)
+    normed = (h * lax.rsqrt(jnp.mean(h * h, axis=-1, keepdims=True) + EPS) * again[...]).astype(BF)
+    angles = column(lanes(prow[...], 0.0)) * freq[...]
+    cos = jnp.cos(angles)
+    low = (lane & 63) < 32
+    sin = jnp.sin(angles) * jnp.where(low, -1.0, 1.0)
+
     for g in range(AHEAD):
         for cp in kv(g):
             cp.start()
+
+    for cp in own_w:
+        cp.wait()
+    gv = gvec[...].astype(F32)
+    gv = jnp.concatenate([gv[i : i + 1] for i in range(16)], axis=1)
+    pad_row = lax.broadcasted_iota(jnp.int32, (4, WIDTH), 0)
+    wdg[0, z, 0:44, :] = dg[...]
+    wdg[0, z, 44:48, :] = jnp.where(pad_row == 0, gv, 0.0).astype(BF)
+    wdg[1, z, 0:44, :] = du[...]
+    wdg[1, z, 44:48, :] = jnp.zeros((4, WIDTH), BF)
+    ddg[1, z] = pltpu.roll(dtail[...].astype(F32), 44, 0).astype(BF)
 
     pl.semaphore_wait(barrier, 19)
 
@@ -183,18 +194,11 @@
     for i in (2, 3, 0, 1):
         w_copy(i).start()
 
-    h = hid[...].astype(F32)
-    normed = (h * lax.rsqrt(jnp.mean(h * h, axis=-1, keepdims=True) + EPS) * again[...]).astype(BF)
-    angles = column(lanes(prow[...], 0.0)) * freq[...]
-    cos = jnp.cos(angles)
-    low = (lane & 63) < 32
-    sin = jnp.sin(angles) * jnp.where(low, -1.0, 1.0)
-
     def rotated(v):
         turned = jnp.where(low, pltpu.roll(v, 96, 1), pltpu.roll(v, 32, 1))
         return (v * cos + turned * sin).astype(BF)
 
-    for cp in first:
+    for cp in first[:2]:
         cp.wait()
     new_k = rotated(dot(normed, wk[...]))
     new_v = dot(normed, wv[...]).astype(BF)
@@ -202,9 +206,11 @@
     out[:, HALF + 128 : HALF + 256] = new_v
     kn[...] = new_k.astype(F32)
     vn[...] = new_v.astype(F32)
-    q = dot(normed, wq[...])
-    for i in range(8):
-        qs[:, i, :] = rotated(q[:, i * 128 : (i + 1) * 128]).astype(F32) * 0.125
+    for i in range(4):
+        first[2 + i].wait()
+        q = dot(normed, wq[:, i * 256 : i * 256 + 256])
+        for j in range(2):
+            qs[:, 2 * i + j, :] = rotated(q[:, j * 128 : j * 128 + 128]).astype(F32) * 0.125
 
     lam_col = jnp.zeros((8, 128), F32)
     rows8 = lax.broadcasted_iota(jnp.int32, (8, 128), 0)
@@ -299,7 +305,7 @@
     def zg_copy(k):
         return remote(own_block, zg.at[z], zs.at[k], zr.at[k], ep=z_ep(k))
 
-    for k in NEAR:
+    for k in FAR:
         g_copy(0, 0, k, 0).start()
         zg_copy(k).start()
     zg[z] = G[b * 4 + a, :, half]
@@ -323,7 +329,7 @@
 
     for ka in NEAR:
         g_arrive(ka, 0)
-        if ka == 1:
+        if ka == NEAR[0]:
             for k in NEAR:
                 g_copy(0, 0, 0, k).start()
     for k in NEAR:
@@ -338,10 +344,11 @@
         to = mate(dy, dx)
         return remote(D.at[to], X.at[p0], xs.at[i], xr.at[i], ep=zb + to)
 
-    def y_copy(dy, dx):
+    def y_copy(dy, dx, n):
         i = dy * 4 + dx
         to = mate(dy, dx)
-        return remote(Y.at[to], R.at[p0], ys.at[i], yr.at[i], ep=zb + to)
+        cols = pl.ds(n * 512, 512)
+        return remote(Y.at[to, :, cols], R.at[p0, :, cols], ys.at[n, i], yr.at[n, i], ep=zb + to)
 
     for k in NEAR:
         ref = zg.at[(z + 4 - k) % 4]
@@ -355,7 +362,7 @@
     X[p0] = D[p0]
 
     for k in NEAR:
-        for ka in (0, 1, 3, 2):
+        for ka in (0, 2, 1, 3):
             g_arrive(ka, k)
     for i in range(4, 8):
         w_wait(i)
@@ -380,18 +387,6 @@
     act_copy = remote(dact.at[0], dact.at[1], das, dar, tp=other)
     act_copy.start()
 
-    def x_share(dy):
-        rows = pl.ds(((y + 4 - dy) % 4) * 4, 4)
-        return remote(X.at[rows], Xo.at[rows], xds.at[dy], xdr.at[dy], tp=other)
-
-    for dy in (0, 1, 3, 2):
-        for dx in range(4):
-            if dy or dx:
-                i = dy * 4 + dx
-                ref = X.at[mate(-dy, -dx)]
-                remote(ref, ref, xs.at[i], xr.at[i], tp=other).wait_recv()
-        x_share(dy).start()
-
     def r1_copy(k):
         to = (b + k) % 4
         return remote(pb.at[to], s1.at[k - 1], r1s.at[k], r1r.at[k], ep=zb + pidx(a, to))
@@ -401,7 +396,7 @@
         return remote(tb.at[to], s2.at[k - 1], r2s.at[k], r2r.at[k], ep=zb + pidx(to, b))
 
     remote(dact.at[0], dact.at[1], das, dar, tp=other).wait_recv()
-    for kb_ in (1, 3, 2, 0):
+    for kb_ in (2, 1, 3, 0):
         g = (b + kb_) % 4
         other_act = jnp.concatenate([dact[1, i * 4 + g] for i in range(4)], axis=0)
         part = dot(dact[0, pl.ds(g * 4, 4)].reshape(128, 256)[:, :192], ddg[c].reshape(192, HALF)) + dot(
@@ -411,53 +406,74 @@
         if kb_:
             r1_copy(kb_).start()
 
+    def x_share(dy):
+        rows = pl.ds(((y + 4 - dy) % 4) * 4, 4)
+        return remote(X.at[rows], Xo.at[rows], xds.at[dy], xdr.at[dy], tp=other)
+
+    for dy in (0, 1, 3, 2):
+        for dx in range(4):
+            if dy or dx:
+                i = dy * 4 + dx
+                ref = X.at[mate(-dy, -dx)]
+                remote(ref, ref, xs.at[i], xr.at[i], tp=other).wait_recv()
+        x_share(dy).start()
+
     for cp in later[1:]:
         cp.wait()
+    own_rows = X[...].reshape(256, HALF)
+    gate_pre = dot_nt(own_rows, eg[:, half])
+    up_pre = dot_nt(own_rows, eu[:, half])
     for dy in (0, 1, 3, 2):
         rows = pl.ds(((y + 4 - dy) % 4) * 4, 4)
         remote(X.at[rows], Xo.at[rows], xds.at[dy], xdr.at[dy], tp=other).wait_recv()
-    own_rows = X[...].reshape(256, HALF)
     other_rows = Xo[...].reshape(256, HALF)
-    gate_pre = dot_nt(own_rows, eg[:, half]) + dot_nt(other_rows, eg[:, other_half])
-    up_pre = dot_nt(own_rows, eu[:, half]) + dot_nt(other_rows, eu[:, other_half])
+    gate_pre = gate_pre + dot_nt(other_rows, eg[:, other_half])
+    up_pre = up_pre + dot_nt(other_rows, eu[:, other_half])
     inner = gate_pre / (1.0 + jnp.exp(-gate_pre)) * up_pre
     abuf[0] = jnp.concatenate([inner, jnp.zeros((256, 32), F32)], axis=1).astype(BF)
     a_copy = remote(abuf.at[0], abuf.at[1], as_, ar, tp=other)
     a_copy.start()
     own_ed = ed[pl.ds(pl.multiple_of(c * 352, 32), 352), :]
     other_ed = ed[pl.ds(pl.multiple_of(other * 352, 32), 352), :]
-    down = dot(abuf[0][:, :352], own_ed)
+    down = [dot(abuf[0][:, :352], own_ed[:, n * 512 : n * 512 + 512]) for n in range(2)]
     remote(abuf.at[0], abuf.at[1], as_, ar, tp=other).wait_recv()
-    down = down + dot(abuf[1][:, :352], other_ed)
-    Y[...] = down.astype(BF).reshape(16, 16, HALF)
-
-    for dy, dx in MATES:
-        y_copy(dy, dx).start()
+
+    for n in range(2):
+        cols = slice(n * 512, n * 512 + 512)
+        part = down[n] + dot(abuf[1][:, :352], other_ed[:, cols])
+        Y[:, :, cols] = part.astype(BF).reshape(16, 16, 512)
+        for dy, dx in MATES:
+            y_copy(dy, dx, n).start()
     R[p0] = Y[p0]
     for k in NEAR:
         r1_copy(k).wait_recv()
     tb[...] = (
         pb[b].astype(F32) + s1[0].astype(F32) + s1[1].astype(F32) + s1[2].astype(F32)
     ).astype(BF)
-    for k in NEAR:
+    for k in FAR:
         r2_copy(k).start()
-    for dy, dx in MATES:
-        i = dy * 4 + dx
-        ref = R.at[mate(-dy, -dx)]
-        remote(ref, ref, ys.at[i], yr.at[i], tp=other).wait_recv()
-    M[...] = dot_tn(selw[...], R[...].reshape(256, HALF)).astype(BF).reshape(4, ROWS, HALF)
-
-    def m_copy(k):
-        return remote(M.at[(z + k) % 4], m_in.at[k - 1], ms.at[k], mr.at[k], ep=z_ep(k))
-
-    for k in NEAR:
-        m_copy(k).start()
+    def m_copy(k, n):
+        cols = pl.ds(n * 512, 512)
+        return remote(
+            M.at[(z + k) % 4, :, cols], m_in.at[k - 1, :, cols], ms.at[n, k], mr.at[n, k], ep=z_ep(k)
+        )
+
+    for n in range(2):
+        for dy, dx in MATES:
+            i = dy * 4 + dx
+            ref = R.at[mate(-dy, -dx), :, pl.ds(n * 512, 512)]
+            remote(ref, ref, ys.at[n, i], yr.at[n, i], tp=other).wait_recv()
+        cols = slice(n * 512, n * 512 + 512)
+        M[:, :, cols] = dot_tn(selw[...], R[:, :, cols].reshape(256, 512)).astype(BF).reshape(4, ROWS, 512)
+        for k in FAR:
+            m_copy(k, n).start()
     for k in NEAR:
         r2_copy(k).wait_recv()
     final = tb[a].astype(F32) + s2[0].astype(F32) + s2[1].astype(F32) + s2[2].astype(F32)
     final = resid[:, half] + final + M[z].astype(F32)
     for k in NEAR:
-        m_copy(k).wait_recv()
+        for n in range(2):
+            m_copy(k, n).wait_recv()
     final = final + m_in[0].astype(F32) + m_in[1].astype(F32) + m_in[2].astype(F32)
     out[:, :HALF] = final.astype(BF)
 
@@ -466,7 +482,8 @@
     for k in NEAR:
         rt_copy(k).wait_send()
         zg_copy(k).wait_send()
-        m_copy(k).wait_send()
+        for n in range(2):
+            m_copy(k, n).wait_send()
         g_copy(0, 0, k, 0).wait_send()
         g_copy(0, 0, 0, k).wait_send()
         r1_copy(k).wait_send()
@@ -475,7 +492,8 @@
             g_copy(i, 0, 0, k).wait_send()
     for dy, dx in MATES:
         x_copy(dy, dx).wait_send()
-        y_copy(dy, dx).wait_send()
+        for n in range(2):
+            y_copy(dy, dx, n).wait_send()
         g_share(dy, dx).wait_send()
     for k in range(4):
         x_share(k).wait_send()
@@ -521,11 +539,11 @@
         V((2, 16, ROWS, 256), BF), V((4, 128, 128), F32), V((256, 128), BF), V((256, 128), BF),
         V((4, 4, ROWS, HALF), BF), V((3, 4, ROWS, HALF), BF), V((4, ROWS, HALF), BF),
         V((3, ROWS, HALF), BF),
-        dma((11,)), dma((2, NGRP)), dma((8,)), dma((8,)), dma, dma,
+        dma((11,)), dma((4,)), dma((2, NGRP)), dma((8,)), dma((8,)), dma, dma,
         dma((4,)), dma((4,)),
         dma((16,)), dma((16,)), dma((16,)), dma((16,)), dma((4,)), dma((4,)), dma((16,)), dma((16,)),
-        dma((4,)), dma((4,)), dma, dma, dma, dma, dma((16,)), dma((16,)),
-        dma((4,)), dma((4,)), dma((4,)), dma((4,)), dma((4,)), dma((4,)),
+        dma((4,)), dma((4,)), dma, dma, dma, dma, dma((2, 16)), dma((2, 16)),
+        dma((4,)), dma((4,)), dma((4,)), dma((4,)), dma((2, 4)), dma((2, 4)),
     ]
     both = pl.pallas_call(
         layer_kernel,

time: 66.4 us -> 66.2 us (level)
  no operation moved by 1% of the time
where the time goes in v6:
time: 66.2 us; the launch traced here: 66 us
  Pallas kernels  64.5 us (97%)
  local copies, waits for them, and re-layouts  0.88 us (1%)
    pallas_call x1, Pallas kernels, per_device(): pl.pallas_call(layer_kernel, name='layer', out_shape=jax.ShapeDtypeStruct...  63.8 us

profile of v6, /device:TPU:0, one launch (start us, length us, event | category | flops | bytes accessed | tf_op | source)
XLA Modules:
  0.0 66.0 jit_solution(11662253594846672997)
XLA Ops:
  0.6 63.8 %layer.1.both = bf16[32,1280]{1,0:T(8,128)(2,1)} custom-call(bf16[32,2048]{1,0:T(8,128)(2,1)} %hid.1, f32[1,128]{1,0:T(1,128)} %constant.2.clone.freq, s32[32]{0:T(128)} %plen.1, s32[1,32]{1,0:T(1,128)} %bitcast.18, f32[1,2048]{1,0:T(1,128)} %bitcast.15, f32[8]{0:T(128)} %lam.1, f32[1,128]{1,0:T(1,128)} %bitcast.21, f32[1,2048]{1,0:T(1,128)} %bitcast.16, ...), custom_call_target="tpu_custom_call" | custom-call | tf_op jit(solution)/shard_map/layer/pallas_call | solution.py:548
  64.5 0.0 copy-start
  64.5 0.9 %copy-done = bf16[32,1280]{1,0:T(8,128)(2,1)S(1)} copy-done((bf16[32,1280]{1,0:T(8,128)(2,1)S(1)}, bf16[32,1280]{1,0:T(8,128)(2,1)}, u32[]{:S(2)}) %copy-start) | copy-done | bytes 81944
  65.3 0.7 split.1
Async XLA Ops:
  64.5 0.9 %copy-start = (bf16[32,1280]{1,0:T(8,128)(2,1)S(1)}, bf16[32,1280]{1,0:T(8,128)(2,1)}, u32[]{:S(2)}) copy-start(bf16[32,1280]{1,0:T(8,128)(2,1)} %layer.1.both) | copy-start | bytes 245764
